TPU v7x, 128 devices: a whole 4x4x4 slice. The times are simulated.
128 devices in a mesh: sp: 16 (over z, x), tp: 8 (over y, core).
Axes of the slice: x: 4, y: 4, z: 4, core: 2. Of those that a mesh axis runs over, the one named last changes fastest.
Arguments:
- query_wide: bfloat16 [12288, 8, 256], P('sp', 'tp'), may hold values from -6 to 6
- key_wide: bfloat16 [12288, 8, 256], P('sp', 'tp'), may hold values from -6 to 6
- value_wide: bfloat16 [12288, 8, 256], P('sp', 'tp'), may hold values from -6 to 6
- query_narrow: bfloat16 [12288, 8, 128], P('sp', 'tp'), may hold values from -6 to 6
- key_narrow: bfloat16 [12288, 8, 128], P('sp', 'tp'), may hold values from -6 to 6
- value_narrow: bfloat16 [12288, 8, 128], P('sp', 'tp'), may hold values from -6 to 6
- mix_lambda: float32 [2, 8], P(None, 'tp'), may hold values from 0.3 to 0.8
- residual_in: bfloat16 [12288, 2048], P(('sp', 'tp')), may hold values from -6 to 6
- out_wide: bfloat16 [2048, 2048], P('tp'), may hold values from -0.109375 to 0.109375
- out_narrow: bfloat16 [1024, 2048], P('tp'), may hold values from -0.109375 to 0.109375
- ffn_gain: float32 [2048], replicated, may hold values from 0.1 to 1.9
- expert_ids: int32 [12288, 2], P(('sp', 'tp')), may hold values from 0 to 127, as said below
- expert_weights: float32 [12288, 2], P(('sp', 'tp')), may hold values from 0.1 to 1
- gate_weight: bfloat16 [128, 2048, 1024], P(('sp', 'tp')), may hold values from -0.125 to 0.125
- up_weight: bfloat16 [128, 2048, 1024], P(('sp', 'tp')), may hold values from -0.125 to 0.125
- down_weight: bfloat16 [128, 1024, 2048], P(('sp', 'tp')), may hold values from -0.1875 to 0.1875
Outputs:
- layer_out: bfloat16 [12288, 2048], P(('sp', 'tp'))
Inputs may be any that keep to these rules, and one draw needn't show every extreme that they name: `expert_ids`: A row's two experts differ and lie in the same group of 4 consecutive experts (32 groups). In each aligned block of 96 rows (the rows of one device) no expert is named by more than 3 rows, and in every block some expert is named by exactly 3 rows.
All inputs are finite; a program needn't handle non-finite values.
Results may differ from a plain program's by a relative error of at most 0.015.
Values may be sent and summed in bfloat16 or wider, within the bound.
A program may use at most 192 MiB of HBM per device.

v0:
```python
import math

import jax
import jax.numpy as jnp
from jax import lax
from jax.sharding import Mesh
from jax.sharding import PartitionSpec as P

TP = ("tp_0", "tp_1")
SP_TP = ("sp", "tp_0", "tp_1")


NEG_FILL = -1e30


def sent_together(arrays, axis, dim, along):
    widths = [a.shape[along] for a in arrays]
    both = jnp.concatenate(arrays, axis=along)
    result = lax.all_gather(both, axis, axis=dim, tiled=True)
    return tuple(jnp.split(result, [sum(widths[:k]) for k in range(1, len(widths))], axis=along))


def cut_along(array, dim, peers):
    before, after = (array.shape[:dim], array.shape[dim + 1 :])
    return jnp.moveaxis(array.reshape(*before, peers, -1, *after), dim, 0)


def laid_out(pieces, dim):
    lengths = list(pieces.shape[1:])
    lengths[dim] *= pieces.shape[0]
    return jnp.moveaxis(pieces, 0, dim).reshape(lengths)


def moved_by_axis(pieces, axes, turns):
    inside = pieces.shape[1:]
    result = pieces.reshape(*(lax.axis_size(a) for a in axes), *inside)
    for k in turns:
        result = lax.all_to_all(result, axes[k], k, k, tiled=True)
    return result.reshape(-1, *inside)


def one_axis_at_a_time(array, axes, turns, split_dim, concat_dim):
    pieces = cut_along(array, split_dim, lax.axis_size(axes))
    return laid_out(moved_by_axis(pieces, axes, turns), concat_dim)


def exchange_in_groups(array, axis, split_dim, concat_dim, work, item_dim, out_dim):

    def moved(group):
        return lax.all_to_all(group, axis, split_axis=split_dim, concat_axis=concat_dim, tiled=True)

    items = jax.tree.leaves(array)[0].shape[item_dim]
    ends = [items * k // 2 for k in range(2 + 1)] if items % 2 == 0 else [0, items]
    groups = [
        jax.tree.map(lambda a: lax.slice_in_dim(a, low, high, axis=item_dim), array)
        for low, high in zip(ends, ends[1:])
    ]
    arrived = [moved(group) for group in groups]
    made = [work(group) for group in arrived]
    return jax.tree.map(lambda *parts: jnp.concatenate(parts, axis=out_dim), *made)


def map_update(state, queries, keys, values, query_pos, key_pos, head_size):
    run_max, run_sum, run_acc = state
    causal = key_pos[None, :] <= query_pos[:, None]
    score_scale = head_size ** (-0.5)
    new_max, new_sum, new_acc = ([], [], [])
    for which_map in range(2):
        lower_edge = which_map * head_size
        scores = (
            jnp.einsum(
                "qhd,khd->hqk",
                queries[..., lower_edge : lower_edge + head_size],
                keys[..., lower_edge : lower_edge + head_size],
                preferred_element_type=jnp.float32,
            )
            * score_scale
        )
        scores = jnp.where(causal[None], scores, NEG_FILL)
        new_peak = jnp.maximum(run_max[which_map], jnp.max(scores, axis=-1))
        factor = jnp.exp(run_max[which_map] - new_peak)
        weights = jnp.where(causal[None], jnp.exp(scores - new_peak[..., None]), 0.0)
        new_sum.append(factor * run_sum[which_map] + jnp.sum(weights, axis=-1))
        new_acc.append(
            factor[..., None] * run_acc[which_map]
            + jnp.einsum(
                "hqk,khv->hqv",
                weights.astype(jnp.bfloat16),
                values,
                preferred_element_type=jnp.float32,
            )
        )
        new_max.append(new_peak)
    return (jnp.stack(new_max), jnp.stack(new_sum), jnp.stack(new_acc))


def finish(state, lam_row):
    run_max, run_sum, run_acc = state
    first_read = run_acc[0] / run_sum[0][..., None]
    second_read = run_acc[1] / run_sum[1][..., None]
    mixed_read = first_read - lam_row[:, None, None] * second_read
    normed = mixed_read * lax.rsqrt(
        jnp.mean(mixed_read * mixed_read, axis=-1, keepdims=True) + 1e-06
    )
    rounded = normed.astype(jnp.bfloat16)
    return jnp.transpose(rounded, (1, 0, 2)).reshape(rounded.shape[1], -1)


def shards(
    query_wide,
    key_wide,
    value_wide,
    query_narrow,
    key_narrow,
    value_narrow,
    mix_lambda,
    residual_in,
    out_wide,
    out_narrow,
    ffn_gain,
    expert_ids,
    expert_weights,
    gate_weight,
    up_weight,
    down_weight,
):
    tok_count, local_heads, _ = query_wide.shape
    size_wide = query_wide.shape[2] // 2
    size_narrow = query_narrow.shape[2] // 2
    offset = lax.axis_index("sp") * tok_count
    query_pos = offset + jnp.arange(tok_count, dtype=jnp.int32)

    def empty_state(values):
        return (
            jnp.full((2, local_heads, tok_count), NEG_FILL, jnp.float32),
            jnp.zeros((2, local_heads, tok_count), jnp.float32),
            jnp.zeros((2, local_heads, tok_count, values.shape[2]), jnp.float32),
        )

    pieces = sent_together((key_wide, value_wide, key_narrow, value_narrow), "sp", 0, 2)

    def visit_piece(current):
        piece_rows = pieces[0].shape[0]
        key_block = math.gcd(piece_rows, 512)
        stacked = tuple(
            (
                member.reshape((piece_rows // key_block, key_block) + member.shape[1:])
                for member in pieces
            )
        )

        def advance(inner_state, block_items):
            number, keys_wide, vals_wide, keys_narrow, vals_narrow = block_items
            key_pos = number * key_block + jnp.arange(key_block, dtype=jnp.int32)
            updated = (
                map_update(
                    inner_state[0], query_wide, keys_wide, vals_wide, query_pos, key_pos, size_wide
                ),
                map_update(
                    inner_state[1],
                    query_narrow,
                    keys_narrow,
                    vals_narrow,
                    query_pos,
                    key_pos,
                    size_narrow,
                ),
            )
            return (updated, None)

        result, _ = lax.scan(
            advance, current, (jnp.arange(piece_rows // key_block, dtype=jnp.int32),) + stacked
        )
        return result

    states = lax.cond(
        jnp.int32(0) > offset + tok_count - 1,
        lambda unchanged: unchanged,
        visit_piece,
        (empty_state(value_wide), empty_state(value_narrow)),
    )
    heads_wide = finish(states[0], mix_lambda[0])
    heads_narrow = finish(states[1], mix_lambda[1])
    tp_size = lax.axis_size(TP)
    local_rows = tok_count // tp_size
    whole_wide, whole_narrow = (
        lax.all_gather(out_wide, TP, axis=0, tiled=True),
        lax.all_gather(out_narrow, TP, axis=0, tiled=True),
    )
    mine_wide, mine_narrow = (
        one_axis_at_a_time(heads_wide, TP, (1, 0), 0, 1),
        one_axis_at_a_time(heads_narrow, TP, (1, 0), 0, 1),
    )
    projected = jnp.dot(mine_wide, whole_wide, preferred_element_type=jnp.float32) + jnp.dot(
        mine_narrow, whole_narrow, preferred_element_type=jnp.float32
    )
    stream = (projected + residual_in.astype(jnp.float32)).astype(jnp.bfloat16)
    stream_f = stream.astype(jnp.float32)
    normed = (
        stream_f
        * lax.rsqrt(jnp.mean(stream_f * stream_f, axis=-1, keepdims=True) + 1e-06)
        * ffn_gain
    ).astype(jnp.bfloat16)
    experts_all = lax.axis_size("sp") * tp_size
    capacity = max(2, 4 * local_rows // experts_all)
    model_width = normed.shape[1]
    flat_expert = expert_ids.reshape(-1)
    expert_hot = (flat_expert[:, None] == jnp.arange(experts_all, dtype=jnp.int32)[None, :]).astype(
        jnp.int32
    )
    slot_rank = jnp.sum((jnp.cumsum(expert_hot, axis=0) - 1) * expert_hot, axis=1)
    flat_slot = flat_expert * capacity + slot_rank
    slot_ids = jnp.arange(experts_all * capacity, dtype=jnp.int32)
    placed = slot_ids[:, None] == flat_slot[None, :]
    dispatch = jnp.any(placed.reshape(experts_all * capacity, local_rows, 2), axis=2).astype(
        jnp.bfloat16
    )
    outgoing = jnp.dot(dispatch, normed, preferred_element_type=jnp.float32).astype(jnp.bfloat16)
    outgoing = outgoing.reshape(experts_all, capacity, model_width)

    def serve_rows(arrived):
        sources, items, width = arrived.shape
        flat_rows = arrived.reshape(sources * items, width)
        gate_part = jnp.dot(flat_rows, gate_weight[0], preferred_element_type=jnp.float32)
        up_part = jnp.dot(flat_rows, up_weight[0], preferred_element_type=jnp.float32)
        hidden = (jax.nn.silu(gate_part) * up_part).astype(jnp.bfloat16)
        result = jnp.dot(hidden, down_weight[0], preferred_element_type=jnp.float32).astype(
            jnp.bfloat16
        )
        return lax.all_to_all(
            result.reshape(sources, items, width), SP_TP, split_axis=0, concat_axis=0, tiled=True
        )

    returned = exchange_in_groups(outgoing, SP_TP, 0, 0, serve_rows, 1, 1)
    slot_hot = (flat_slot[:, None] == slot_ids[None, :]).astype(
        jnp.float32
    ) * expert_weights.reshape(-1)[:, None]
    combine = jnp.sum(slot_hot.reshape(local_rows, 2, experts_all * capacity), axis=1)
    summed = jnp.dot(
        combine, returned.reshape(experts_all * capacity, model_width).astype(jnp.float32)
    )
    return (stream_f + summed).astype(jnp.bfloat16)


def solution(mesh):
    finer = Mesh(mesh.devices.reshape(mesh.shape["sp"], 4, 2), ("sp", "tp_0", "tp_1"))
    placed = (
        P("sp", TP, None),
        P("sp", TP, None),
        P("sp", TP, None),
        P("sp", TP, None),
        P("sp", TP, None),
        P("sp", TP, None),
        P(None, TP),
        P(SP_TP, None),
        P(TP, None),
        P(TP, None),
        P(),
        P(SP_TP, None),
        P(SP_TP, None),
        P(SP_TP, None, None),
        P(SP_TP, None, None),
        P(SP_TP, None, None),
    )
    return jax.shard_map(
        shards, mesh=finer, in_specs=placed, out_specs=P(SP_TP, None), check_vma=False
    )
```

profile of v0, /device:TPU:1, one launch (start us, length us, event | category | flops | bytes accessed | tf_op | source)
XLA Modules:
  0.0 600.0 jit_solution(8336689314368046976)
XLA Ops:
  6.5 2.4 pad_maximum_fusion.6
  12.2 122.4 %all-gather.4.cloned.1.call-done = bf16[12288,1,768]{2,0,1:T(8,128)(2,1)} async-done(((bf16[768,1,768]{2,0,1:T(8,128)(2,1)}), bf16[12288,1,768]{2,0,1:T(8,128)(2,1)}) %all-gather.4.cloned.1.call-update) | async-done | bytes 18874384 | tf_op jit(solution)/shard_map/all_gather | solution.py:19
  134.6 313.0 %conditional.1 = (f32[2,1,768]{2,1,0:T(1,128)S(1)}, f32[2,1,768,256]{3,2,1,0:T(8,128)S(1)}, f32[2,1,768]{2,1,0:T(1,128)S(1)}, f32[2,1,768,128]{3,2,1,0:T(8,128)S(1)}) conditional(s32[]{:T(128)} %convert_element_type.60, (bf16[12288,1,768]{2,0,1:T(8,128)(2,1)}, s32[]{:T(128)}, s32[768]{0:T(1024)S(1)}, bf16[768,1,256]{2,0,1:T(8,128)(2,1)S(1)}, ...), branch_computations={%region_0.11_spmd, %region_11.12_spmd} | conditional | flops 925453568 | bytes 71843312 | solution.py:176
  134.6 10.1 %fusion.97 = (bf16[12288,1,256]{2,0,1:T(8,128)(2,1)}, bf16[12288,1,256]{2,0,1:T(8,128)(2,1)}) fusion(bf16[12288,1,768]{2,0,1:T(8,128)(2,1)} %get-tuple-element.102), kind=kLoop, calls=%fused_computation.163 | loop fusion | bytes 25165824 | tf_op jit(solution)/shard_map/split | solution.py:20
  144.7 5.5 fusion.96
  150.6 297.0 %while.19 = (s32[]{:T(128)}, f32[2,1,768]{2,1,0:T(1,128)S(1)}, f32[2,1,768]{2,1,0:T(1,128)S(1)}, f32[2,1,768,256]{3,2,1,0:T(8,128)S(1)}, f32[2,1,768]{2,1,0:T(1,...) while((s32[]{:T(128)}, f32[2,1,768]{2,1,0:T(1,128)S(1)}, ...), condition=%wide.region_10.10_spmd, body=%wide.region_1.9_spmd.sunk | while | flops 925452800 | bytes 31311040 | solution.py:171
  453.1 4.8 all_to_all.30
  457.9 3.8 all-to-all-start.2
  462.8 3.9 all-to-all-start.1
  467.5 6.4 %all-to-all-done.1 = bf16[4,2,96,256]{3,2,1,0:T(8,128)(2,1)S(1)} async-done(((bf16[4,2,96,256]{3,2,1,0:T(8,128)(2,1)}), bf16[4,2,96,256]{3,2,1,0:T(8,128)(2,1)S(1)}, u32[]{:S(2)}, u32[]{:S(2)}) %all-to-all-start.1) | async-done | bytes 393248 | tf_op jit(solution)/shard_map/all_to_all | solution.py:38
  473.9 3.5 all-to-all-start.3
  477.6 4.9 fusion.101
  482.5 3.2 multiply_reduce_fusion
  485.7 1.8 convolution_convert_fusion
  487.5 4.0 reshape.683
  491.5 39.0 %all_to_all.31 = bf16[128,3,2048]{2,1,0:T(4,128)(2,1)} all-to-all(bf16[128,3,2048]{2,1,0:T(4,128)(2,1)S(1)} %reshape.683), channel_id=1, replica_groups=mesh['sp'=16,'tp_0'=4,'tp_1'=2] {'sp','tp_0','tp_1'}, dimensions={0} | all-to-all | bytes 3145728 | tf_op jit(solution)/shard_map/all_to_all | solution.py:50
  530.5 3.9 reshape.684
  534.4 5.1 fusion.60
  539.5 8.6 %fusion.62 = bf16[384,2048]{1,0:T(8,128)(2,1)} fusion(bf16[1,1024,2048]{2,1,0:T(8,128)(2,1)} %param.35, f32[384,1024]{1,0:T(8,128)} %fusion.60, bf16[384,2048]{1,0:T(8,128)(2,1)S(1)} %reshape.684, bf16[1,2048,1024]{2,1,0:T(8,128)(2,1)} %param.34), kind=kOutput, calls=%fused_computation.104 | convolution fusion | flops 3224371200 | bytes 13107200 | tf_op jit(solution)/shard_map/dot_general | solution.py:227
  548.1 5.1 reshape.685
  553.3 4.9 all-to-all-start.5
  558.3 30.1 %all-to-all-done.5 = bf16[128,3,2048]{2,1,0:T(4,128)(2,1)S(1)} async-done(((bf16[128,3,2048]{2,1,0:T(4,128)(2,1)}), bf16[128,3,2048]{2,1,0:T(4,128)(2,1)S(1)}, u32[]{:S(2)}, u32[]{:S(2)}) %all-to-all-start.5) | async-done | bytes 1572896 | tf_op jit(solution)/shard_map/all_to_all | solution.py:230
  588.4 2.5 reshape.686
  590.9 2.6 fusion.66
  (697 shorter events, 287.0 us)
Async XLA Ops:
  6.5 128.1 %all-gather.4.cloned.1.call-start = ((), (), s32[]{:S(2)}) async-start(), calls=%async_computation.6 | async-start | bytes 20054016 | tf_op jit(solution)/shard_map/all_gather | solution.py:19
  9.0 1.6 copy-start.3
  9.0 2.5 copy-start.4
  9.0 125.6 %copy-start.1 = (bf16[768,1,128]{2,0,1:T(8,128)(2,1)S(1)}, bf16[768,1,128]{2,0,1:T(8,128)(2,1)}, u32[]{:S(2)}) copy-start(bf16[768,1,128]{2,0,1:T(8,128)(2,1)} %param.23) | copy-start | bytes 589828
  9.0 125.6 %copy-start.6 = (bf16[768,1,256]{2,0,1:T(8,128)(2,1)S(1)}, bf16[768,1,256]{2,0,1:T(8,128)(2,1)}, u32[]{:S(2)}) copy-start(bf16[768,1,256]{2,0,1:T(8,128)(2,1)} %param.20) | copy-start | bytes 1179652
  9.0 468.5 %all-gather.6.cloned.1.call-start = ((), (), s32[]{:S(2)}) async-start(), calls=%async_computation.7 | async-start | bytes 9437184 | tf_op jit(solution)/shard_map/all_gather | solution.py:187
  9.8 472.7 %all-gather.8.cloned.1.call-start = ((), (), s32[]{:S(2)}) async-start(), calls=%async_computation.8 | async-start | bytes 4718592 | tf_op jit(solution)/shard_map/all_gather | solution.py:188
  457.9 4.9 all-to-all-start.2
  462.8 11.1 %all-to-all-start.1 = ((bf16[4,2,96,256]{3,2,1,0:T(8,128)(2,1)}), bf16[4,2,96,256]{3,2,1,0:T(8,128)(2,1)S(1)}, u32[]{:S(2)}, u32[]{:S(2)}) async-start(bf16[4,2,96,256]{3,2,1,0:T(8,128)(2,1)} %copy.93), calls=%async_computation.1 | async-start | bytes 786432 | tf_op jit(solution)/shard_map/all_to_all | solution.py:38
  473.9 8.5 %all-to-all-start.3 = ((bf16[4,2,96,128]{3,2,1,0:T(8,128)(2,1)}), bf16[4,2,96,128]{3,2,1,0:T(8,128)(2,1)S(1)}, u32[]{:S(2)}, u32[]{:S(2)}) async-start(bf16[4,2,96,128]{3,2,1,0:T(8,128)(2,1)} %copy.96), calls=%async_computation.3 | async-start | bytes 393216 | tf_op jit(solution)/shard_map/all_to_all | solution.py:38
  477.5 4.9 copy-start
  482.5 3.2 copy-start.2
  553.2 4.9 copy-start.5
  553.3 35.1 %all-to-all-start.5 = ((bf16[128,3,2048]{2,1,0:T(4,128)(2,1)}), bf16[128,3,2048]{2,1,0:T(4,128)(2,1)S(1)}, u32[]{:S(2)}, u32[]{:S(2)}) async-start(bf16[128,3,2048]{2,1,0:T(4,128)(2,1)} %reshape.685), calls=%async_computation.5 | async-start | bytes 4194304 | tf_op jit(solution)/shard_map/all_to_all | solution.py:230
Sparse Core Ops, SparseCore 0:
  9.5 125.0 all-gather.3
  136.3 49.8 all-gather.5
  187.9 32.2 all-gather.7
where the time goes:
time: 605 us; the launch traced here: 600 us
  matrix products  206 us (34%)
  waiting for transfers between devices  161 us (27%)
  local copies, waits for them, and re-layouts  98.1 us (16%)
  blocking collectives  43.8 us (7%)
  other arithmetic  40.9 us (7%)
  loops' own time  21 us (3%)
  starting transfers between devices  16.2 us (3%)
  between operations  13.4 us (2%)
    dot_general x96, matrix products, map_update(): jnp.einsum('hqk,khv->hqv', weights.astype(jnp.bfloat16), values, preferre...  142 us
    all_gather x1, waiting for transfers between devices, sent_together(): result = lax.all_gather(both, axis, axis=dim, tiled=True)  122 us
    squeeze x48, local copies, waits for them, and re-layouts, visit_piece(): lax.scan(advance, current, (jnp.arange(piece_rows // key_block, dtype=jnp...  45.5 us
    all_to_all x1, blocking collectives, moved(): lax.all_to_all(group, axis, split_axis=split_dim, concat_axis=concat_dim,...  39 us
    dot_general x96, matrix products, map_update(): jnp.einsum('qhd,khd->hqk', queries[..., lower_edge:lower_edge + head_size...  38 us
    all_to_all x1, waiting for transfers between devices, serve_rows(): lax.all_to_all(result.reshape(sources, items, width), SP_TP, split_axis=0...  30.1 us
    reduce_sum x24, other arithmetic, map_update(): new_sum.append(factor * run_sum[which_map] + jnp.sum(weights, axis=-1))  27.3 us
    another operation x1, loops' own time, visit_piece(): lax.scan(advance, current, (jnp.arange(piece_rows // key_block, dtype=jnp...  21 us
  transfers between devices with their start and end apart: 7, of which 4 were waited for; matrix products, arithmetic and copies ran while one was open for 51% of the time, Pallas kernels for 0%

commit v1 on v0

v1 whole, which is shorter than its diff:
```python
import functools
import jax
import jax.numpy as jnp
from jax import lax
from jax.experimental import pallas as pl
from jax.experimental.pallas import tpu as pltpu
from jax.sharding import Mesh
from jax.sharding import PartitionSpec as P

TP = ("y", "c")
SP = ("z", "x")
SP_TP = ("z", "x", "y", "c")

NEG = -1e30
LOG2E = 1.4426950408889634


TQ = 256


def flash_body(pos_ref, *refs, d, dv, nq, nk):
    q_in = refs[:nq]
    kv_in = refs[nq:nq + nk]
    acc_out, stat_out = refs[nq + nk:nq + nk + 2]
    q_s, k_s, v_s, qt_s, vt_s, s_a, s_b, t_a, t_b, p_scr, acc, m_s, l_s, st_buf, tab, sems, out_sem = refs[nq + nk + 2:]
    rows = q_in[0].shape[0]
    half = rows // 2
    copies = []
    for n, src in enumerate(q_in):
        copies.append(pltpu.make_async_copy(src, q_s.at[pl.ds(n * rows, rows)], sems.at[n]))
    for n, src in enumerate(kv_in):
        for h in range(2):
            at = h * nk * half + n * half
            part = src.at[pl.ds(h * half, half)]
            copies.append(pltpu.make_async_copy(part.at[:, pl.ds(0, 2 * d)], k_s.at[pl.ds(at, half)], sems.at[nq + 4 * n + 2 * h]))
            copies.append(pltpu.make_async_copy(part.at[:, pl.ds(2 * d, dv)], v_s.at[pl.ds(at, half)], sems.at[nq + 4 * n + 2 * h + 1]))
    for c in copies:
        c.start()
    for c in copies:
        c.wait()
    scale = d ** (-0.5) * LOG2E
    total_q, total_k = nq * rows, nk * rows
    TK = rows
    tiles_q, tiles_k = total_q // TQ, total_k // TK

    def turn(i, _):
        r = pl.multiple_of(i * rows, rows)
        qt_s[:, pl.ds(r, rows)] = q_s[pl.ds(r, rows)].T
        vt_s[:, pl.ds(r, rows)] = v_s[pl.ds(r, rows)].T
        return 0
    lax.fori_loop(0, nq, turn, 0)

    def list_q(qi, n):
        per = rows // TQ
        qp = pos_ref[qi // per] + (qi % per) * TQ

        def list_k(kj, carry):
            n, first = carry
            p0, p1 = pos_ref[nq + 2 * kj], pos_ref[nq + 2 * kj + 1]
            hi, lo = jnp.maximum(p0, p1), jnp.minimum(p0, p1)
            full = hi + half - 1 <= qp
            some = lo <= qp + TQ - 1
            tab[0, n] = qi
            tab[1, n] = kj
            tab[2, n] = jnp.where(full, 0, 1)
            tab[3, n] = first
            return n + some.astype(jnp.int32), jnp.where(some, 0, first)
        m, first = lax.fori_loop(0, tiles_k, list_k, (n, 1))

        @pl.when(m == n)
        def _():
            tab[0, n] = qi
            tab[1, n] = 0
            tab[2, n] = 1
            tab[3, n] = 1
        return jnp.maximum(m, n + 1)
    steps = lax.fori_loop(0, tiles_q, list_q, 0)
    tab[3, steps] = 1

    CH = 256

    def read(i, s_buf, t_buf):
        q0 = pl.multiple_of(tab[0, i] * TQ, TQ)
        k0 = pl.multiple_of(tab[1, i] * TK, TK)
        for w in range(2):
            qt = qt_s[w * d:(w + 1) * d, pl.ds(q0, TQ)]
            top = None
            for c in range(TK // CH):
                k = k_s[pl.ds(k0 + c * CH, CH), w * d:(w + 1) * d]
                s = jnp.dot(k, qt, preferred_element_type=jnp.float32)
                s_buf[w, c * CH:(c + 1) * CH] = s
                m8 = jnp.max(s.reshape(CH // 8, 8, TQ), axis=0)
                top = m8 if top is None else jnp.maximum(top, m8)
            t_buf[w] = top

    def mask(i, s_buf, t_buf):
        per = rows // TQ
        qi, kj = tab[0, i], tab[1, i]
        qp = pos_ref[qi // per] + (qi % per) * TQ
        CM = 128
        t_buf[...] = jnp.full_like(t_buf, NEG)

        def chunk(c, _):
            r = pl.multiple_of(c * CM, CM)
            late = (c >= half // CM).astype(jnp.int32)
            k0 = pos_ref[nq + 2 * kj + late] + (c - late * (half // CM)) * CM
            keep = lax.broadcasted_iota(jnp.int32, (CM, TQ), 0) - lax.broadcasted_iota(jnp.int32, (CM, TQ), 1) <= qp - k0
            for w in range(2):
                s = jnp.where(keep, s_buf[w, pl.ds(r, CM)], NEG)
                s_buf[w, pl.ds(r, CM)] = s
                t_buf[w] = jnp.maximum(t_buf[w], jnp.max(s.reshape(CM // 8, 8, TQ), axis=0))
            return 0
        lax.fori_loop(0, TK // CM, chunk, 0)

    def weigh(i, par, s_buf, t_buf):
        k0 = pl.multiple_of(tab[1, i] * TK, TK)
        for w in range(2):
            old = m_s[w:w + 1]
            new = jnp.maximum(old, jnp.max(t_buf[w], axis=0, keepdims=True) * scale)
            f = jnp.exp2(old - new)
            m_s[w:w + 1] = new
            tot = None
            for c in range(TK // CH):
                p = jnp.exp2(s_buf[w, c * CH:(c + 1) * CH] * scale - new)
                t8 = jnp.sum(p.reshape(CH // 8, 8, TQ), axis=0)
                tot = t8 if tot is None else tot + t8
                p_scr[w, c * CH:(c + 1) * CH] = p.astype(jnp.bfloat16)
            o = jnp.dot(vt_s[:, pl.ds(k0, TK)], p_scr[w], preferred_element_type=jnp.float32)
            l_s[w] = l_s[w] * f + tot
            acc[par, w] = acc[par, w] * f + o

    def out_copies(qi, par):
        q0 = pl.multiple_of(qi * TQ, TQ)
        return (
            pltpu.make_async_copy(acc.at[par], acc_out.at[:, :, pl.ds(q0, TQ)], out_sem.at[par, 0]),
            pltpu.make_async_copy(st_buf.at[par], stat_out.at[:, pl.ds(q0, TQ)], out_sem.at[par, 1]),
        )

    def advance(i, cur, nxt):
        qi = tab[0, i]
        par = qi % 2

        @pl.when(tab[3, i] == 1)
        def _():
            @pl.when(qi >= 2)
            def _():
                for c in out_copies(qi - 2, par):
                    c.wait()
            m_s[...] = jnp.full_like(m_s, NEG)
            l_s[...] = jnp.zeros_like(l_s)
            acc[par] = jnp.zeros((2, dv, TQ), jnp.float32)

        @pl.when(tab[2, i] == 1)
        def _():
            mask(i, *cur)
        read(jnp.minimum(i + 1, steps - 1), *nxt)
        weigh(i, par, *cur)

        @pl.when(tab[3, i + 1] == 1)
        def _():
            st_buf[par, 0:2] = m_s[...]
            for w in range(2):
                st_buf[par, 2 + w:3 + w] = jnp.sum(l_s[w], axis=0, keepdims=True)
            for c in out_copies(qi, par):
                c.start()

    one, two = (s_a, t_a), (s_b, t_b)
    read(0, *one)

    def pair(n, _):
        advance(2 * n, one, two)

        @pl.when(2 * n + 1 < steps)
        def _():
            advance(2 * n + 1, two, one)
        return 0
    lax.fori_loop(0, (steps + 1) // 2, pair, 0)
    for qi in (tiles_q - 2, tiles_q - 1):
        for c in out_copies(qi, qi % 2):
            c.wait()


def flash(pos, qs, kvs, d, dv, units=9.5):
    rows = qs[0].shape[0]
    nq, nk = len(qs), len(kvs)
    total, keys = nq * rows, nk * rows
    any_ = pl.BlockSpec(memory_space=pl.ANY)
    flops = int(units * rows * rows * 2 * (d + dv) * 2)
    return pl.pallas_call(
        functools.partial(flash_body, d=d, dv=dv, nq=nq, nk=nk),
        out_shape=(jax.ShapeDtypeStruct((2, dv, total), jnp.float32), jax.ShapeDtypeStruct((4, total), jnp.float32)),
        in_specs=[pl.BlockSpec(memory_space=pltpu.SMEM)] + [any_] * (nq + nk),
        out_specs=(any_, any_),
        scratch_shapes=[
            pltpu.VMEM((total, 2 * d), jnp.bfloat16),
            pltpu.VMEM((keys, 2 * d), jnp.bfloat16),
            pltpu.VMEM((keys, dv), jnp.bfloat16),
            pltpu.VMEM((2 * d, total), jnp.bfloat16),
            pltpu.VMEM((dv, keys), jnp.bfloat16),
            pltpu.VMEM((2, rows, TQ), jnp.float32),
            pltpu.VMEM((2, rows, TQ), jnp.float32),
            pltpu.VMEM((2, 8, TQ), jnp.float32),
            pltpu.VMEM((2, 8, TQ), jnp.float32),
            pltpu.VMEM((2, rows, TQ), jnp.bfloat16),
            pltpu.VMEM((2, 2, dv, TQ), jnp.float32),
            pltpu.VMEM((2, TQ), jnp.float32),
            pltpu.VMEM((2, 8, TQ), jnp.float32),
            pltpu.VMEM((2, 4, TQ), jnp.float32),
            pltpu.SMEM((4, total // TQ * (keys // rows) + 1), jnp.int32),
            pltpu.SemaphoreType.DMA((nq + 4 * nk,)),
            pltpu.SemaphoreType.DMA((2, 2)),
        ],
        name="flash_wide" if d == 128 else "flash_narrow",
        cost_estimate=pl.CostEstimate(flops=flops, bytes_accessed=total * (dv * 8 + 2 * d * 4 + dv * 2), transcendentals=0),
        compiler_params=pltpu.CompilerParams(vmem_limit_bytes=50 * 2**20),
    )(pos, *qs, *kvs)


def mix_body(lam_ref, acc_ref, own_ref, *refs, row):
    peers, out_ref = refs[:-1], refs[-1]
    stats = [own_ref[...]] + [r[...] for r in peers]
    weights = []
    for w in range(2):
        peaks = [s[w:w + 1] for s in stats]
        sums = [s[2 + w:3 + w] for s in stats]
        top = functools.reduce(jnp.maximum, peaks)
        total = sum(l * jnp.exp2(m - top) for m, l in zip(peaks, sums))
        weights.append(jnp.exp2(peaks[0] - top) / total)
    mixed = acc_ref[0] * weights[0] - acc_ref[1] * (weights[1] * lam_ref[row, 0])
    out_ref[...] = mixed.T.astype(jnp.bfloat16)


def mix(lam, acc, own, peers, row):
    _, dv, total = acc.shape
    B = 512
    return pl.pallas_call(
        functools.partial(mix_body, row=row),
        grid=(total // B,),
        out_shape=jax.ShapeDtypeStruct((total, dv), jnp.bfloat16),
        in_specs=[pl.BlockSpec(memory_space=pltpu.SMEM), pl.BlockSpec((2, dv, B), lambda i: (0, 0, i))]
        + [pl.BlockSpec((4, B), lambda i: (0, i))] * (1 + len(peers)),
        out_specs=pl.BlockSpec((B, dv), lambda i: (i, 0)),
        name="mix_wide" if dv == 256 else "mix_narrow",
        cost_estimate=pl.CostEstimate(flops=total * dv * 4, bytes_accessed=total * dv * 10, transcendentals=0),
    )(lam, acc, own, *peers)


def ring(axis, t):
    return lambda a: lax.ppermute(a, axis, [(i, (i + t) % 4) for i in range(4)])


SHIFTS = (0, 1, 3, 2)


def gather_parts(q, k, v):
    half = q.shape[0] // 2
    kv = jnp.concatenate([k, v], axis=1)
    swapped = lax.ppermute(kv[half:], "z", [(i, 3 - i) for i in range(4)])
    mine = jnp.concatenate([kv[:half], swapped], axis=0)
    kvs = [mine] + [ring("x", t)(mine) for t in SHIFTS[1:]]
    qs = [q] + [ring("z", t)(q) for t in SHIFTS[1:]]
    return qs, kvs


def positions():
    z, x = lax.axis_index("z"), lax.axis_index("x")
    return jnp.stack([jnp.int32(p) for p in positions_of(z, x)])


def positions_of(z, x, rows=768):
    half = rows // 2
    qp = [(4 * ((z + 4 - t) % 4) + x) * rows for t in SHIFTS]
    ns = [(x + 4 - t) % 4 for t in SHIFTS]
    return qp + [(4 * z + n) * rows for n in ns] + [(4 * (3 - z) + n) * rows + half for n in ns]


def combine(lam, acc, stat, row):
    rows = acc.shape[2] // 4
    peers = [ring("z", t)(stat_roll(stat, t)) for t in (1, 2, 3)]
    part = mix(lam, acc, stat, peers, row)
    slot = {t: i for i, t in enumerate(SHIFTS)}
    total = part[:rows].astype(jnp.float32)
    for t in (1, 3, 2):
        i = slot[t]
        back = lax.ppermute(part[i * rows:(i + 1) * rows], "z", [(j, (j - t) % 4) for j in range(4)])
        total = total + back.astype(jnp.float32)
    return (total * lax.rsqrt(jnp.mean(total * total, axis=-1, keepdims=True) + 1e-6)).astype(jnp.bfloat16)


def stat_roll(stat, t):
    rows = stat.shape[1] // 4
    slot = {s: i for i, s in enumerate(SHIFTS)}
    return jnp.concatenate([stat[:, slot[(s - t) % 4] * rows:(slot[(s - t) % 4] + 1) * rows] for s in SHIFTS], axis=1)


def attention(qw, kw, vw, qn, kn, vn, lam):
    qw, kw, vw, qn, kn, vn = (a[:, 0] for a in (qw, kw, vw, qn, kn, vn))
    pos = positions()
    qns, kvns = gather_parts(qn, kn, vn)
    qws, kvws = gather_parts(qw, kw, vw)
    accn, stn = flash(pos, qns, kvns, 64, 128)
    accw, stw = flash(pos, qws, kvws, 128, 256)
    heads_n = combine(lam, accn, stn, 1)
    heads_w = combine(lam, accw, stw, 0)
    return heads_w, heads_n


def cut_along(array, dim, peers):
    before, after = (array.shape[:dim], array.shape[dim + 1 :])
    return jnp.moveaxis(array.reshape(*before, peers, -1, *after), dim, 0)


def laid_out(pieces, dim):
    lengths = list(pieces.shape[1:])
    lengths[dim] *= pieces.shape[0]
    return jnp.moveaxis(pieces, 0, dim).reshape(lengths)


def moved_by_axis(pieces, axes, turns):
    inside = pieces.shape[1:]
    result = pieces.reshape(*(lax.axis_size(a) for a in axes), *inside)
    for k in turns:
        result = lax.all_to_all(result, axes[k], k, k, tiled=True)
    return result.reshape(-1, *inside)


def one_axis_at_a_time(array, axes, turns, split_dim, concat_dim):
    pieces = cut_along(array, split_dim, lax.axis_size(axes))
    return laid_out(moved_by_axis(pieces, axes, turns), concat_dim)


def exchange_in_groups(array, axis, split_dim, concat_dim, work, item_dim, out_dim):

    def moved(group):
        return lax.all_to_all(group, axis, split_axis=split_dim, concat_axis=concat_dim, tiled=True)

    items = jax.tree.leaves(array)[0].shape[item_dim]
    ends = [items * k // 2 for k in range(2 + 1)] if items % 2 == 0 else [0, items]
    groups = [
        jax.tree.map(lambda a: lax.slice_in_dim(a, low, high, axis=item_dim), array)
        for low, high in zip(ends, ends[1:])
    ]
    arrived = [moved(group) for group in groups]
    made = [work(group) for group in arrived]
    return jax.tree.map(lambda *parts: jnp.concatenate(parts, axis=out_dim), *made)


def shards(
    query_wide,
    key_wide,
    value_wide,
    query_narrow,
    key_narrow,
    value_narrow,
    mix_lambda,
    residual_in,
    out_wide,
    out_narrow,
    ffn_gain,
    expert_ids,
    expert_weights,
    gate_weight,
    up_weight,
    down_weight,
):
    tok_count, local_heads, _ = query_wide.shape
    heads_wide, heads_narrow = attention(
        query_wide, key_wide, value_wide, query_narrow, key_narrow, value_narrow, mix_lambda
    )
    tp_size = lax.axis_size(TP)
    local_rows = tok_count // tp_size
    whole_wide, whole_narrow = (
        lax.all_gather(out_wide, TP, axis=0, tiled=True),
        lax.all_gather(out_narrow, TP, axis=0, tiled=True),
    )
    mine_wide, mine_narrow = (
        one_axis_at_a_time(heads_wide, TP, (1, 0), 0, 1),
        one_axis_at_a_time(heads_narrow, TP, (1, 0), 0, 1),
    )
    projected = jnp.dot(mine_wide, whole_wide, preferred_element_type=jnp.float32) + jnp.dot(
        mine_narrow, whole_narrow, preferred_element_type=jnp.float32
    )
    stream = (projected + residual_in.astype(jnp.float32)).astype(jnp.bfloat16)
    stream_f = stream.astype(jnp.float32)
    normed = (
        stream_f
        * lax.rsqrt(jnp.mean(stream_f * stream_f, axis=-1, keepdims=True) + 1e-06)
        * ffn_gain
    ).astype(jnp.bfloat16)
    experts_all = lax.axis_size(SP) * tp_size
    capacity = max(2, 4 * local_rows // experts_all)
    model_width = normed.shape[1]
    flat_expert = expert_ids.reshape(-1)
    expert_hot = (flat_expert[:, None] == jnp.arange(experts_all, dtype=jnp.int32)[None, :]).astype(
        jnp.int32
    )
    slot_rank = jnp.sum((jnp.cumsum(expert_hot, axis=0) - 1) * expert_hot, axis=1)
    flat_slot = flat_expert * capacity + slot_rank
    slot_ids = jnp.arange(experts_all * capacity, dtype=jnp.int32)
    placed = slot_ids[:, None] == flat_slot[None, :]
    dispatch = jnp.any(placed.reshape(experts_all * capacity, local_rows, 2), axis=2).astype(
        jnp.bfloat16
    )
    outgoing = jnp.dot(dispatch, normed, preferred_element_type=jnp.float32).astype(jnp.bfloat16)
    outgoing = outgoing.reshape(experts_all, capacity, model_width)

    def serve_rows(arrived):
        sources, items, width = arrived.shape
        flat_rows = arrived.reshape(sources * items, width)
        gate_part = jnp.dot(flat_rows, gate_weight[0], preferred_element_type=jnp.float32)
        up_part = jnp.dot(flat_rows, up_weight[0], preferred_element_type=jnp.float32)
        hidden = (jax.nn.silu(gate_part) * up_part).astype(jnp.bfloat16)
        result = jnp.dot(hidden, down_weight[0], preferred_element_type=jnp.float32).astype(
            jnp.bfloat16
        )
        return lax.all_to_all(
            result.reshape(sources, items, width), SP_TP, split_axis=0, concat_axis=0, tiled=True
        )

    returned = exchange_in_groups(outgoing, SP_TP, 0, 0, serve_rows, 1, 1)
    slot_hot = (flat_slot[:, None] == slot_ids[None, :]).astype(
        jnp.float32
    ) * expert_weights.reshape(-1)[:, None]
    combine = jnp.sum(slot_hot.reshape(local_rows, 2, experts_all * capacity), axis=1)
    summed = jnp.dot(
        combine, returned.reshape(experts_all * capacity, model_width).astype(jnp.float32)
    )
    return (stream_f + summed).astype(jnp.bfloat16)


def solution(mesh):
    finer = Mesh(mesh.devices.reshape(4, 4, 4, 2), ("z", "x", "y", "c"))
    placed = (
        P(SP, TP, None),
        P(SP, TP, None),
        P(SP, TP, None),
        P(SP, TP, None),
        P(SP, TP, None),
        P(SP, TP, None),
        P(None, TP),
        P(SP_TP, None),
        P(TP, None),
        P(TP, None),
        P(),
        P(SP_TP, None),
        P(SP_TP, None),
        P(SP_TP, None, None),
        P(SP_TP, None, None),
        P(SP_TP, None, None),
    )
    return jax.shard_map(
        shards, mesh=finer, in_specs=placed, out_specs=P(SP_TP, None), check_vma=False
    )
```

time: 605 us -> 319 us (0.53)
  matrix products: 206 us -> 26.2 us
  waiting for transfers between devices: 161 us -> 76.6 us
  local copies, waits for them, and re-layouts: 98.1 us -> 23.1 us
  Pallas kernels: 0 us -> 53.8 us
  starting transfers between devices: 16.2 us -> 66.8 us
  other arithmetic: 40.9 us -> 5.41 us
  loops' own time: 21 us -> 0 us
  blocking collectives: 43.8 us -> 51.6 us
    dot_general x192 -> x0, matrix products: 180 us -> none  [the longest x96 142 us: map_update(): jnp.einsum('hqk,khv->hqv', weights.astype(jnp.bfloat16), values, preferre...]
    all_gather x1 -> x0, waiting for transfers between devices: 122 us -> none  [sent_together(): result = lax.all_gather(both, axis, axis=dim, tiled=True)]
    pallas_call x0 -> x4, Pallas kernels: none -> 53.8 us  [the longest x2 42.6 us: flash(): pl.pallas_call(functools.partial(flash_body, d=d, dv=dv, nq=nq, nk=nk), o...]
    ppermute x0 -> x26, starting transfers between devices: none -> 50.5 us  [the longest x18 34.9 us: ring(): return lambda a: lax.ppermute(a, axis, [(i, (i + t) % 4) for i in range(4)])]
    squeeze x48 -> x0, local copies, waits for them, and re-layouts: 45.5 us -> none  [visit_piece(): lax.scan(advance, current, (jnp.arange(piece_rows // key_block, dtype=jnp...]
    ppermute x0 -> x26, waiting for transfers between devices: none -> 38.1 us  [the longest x18 17.9 us: ring(): return lambda a: lax.ppermute(a, axis, [(i, (i + t) % 4) for i in range(4)])]
    reduce_sum x26 -> x2, other arithmetic: 29.4 us -> 1.48 us  [combine(): jnp.mean(total * total, axis=-1, keepdims=True) + 1e-06]
    another operation x2 -> x0, loops' own time: 21 us -> none  [the longest x1 21 us: visit_piece(): lax.scan(advance, current, (jnp.arange(piece_rows // key_block, dtype=jnp...]
  transfers between devices with their start and end apart: 7 -> 32, of which waited for: 4 -> 11; matrix products, arithmetic and copies ran while one was open for 51% -> 5% of each run, Pallas kernels for 0% -> 17%
where the time goes in v1:
time: 319 us; the launch traced here: 317 us
  waiting for transfers between devices  76.6 us (24%)
  starting transfers between devices  66.8 us (21%)
  Pallas kernels  53.8 us (17%)
  blocking collectives  51.6 us (16%)
  matrix products  26.2 us (8%)
  local copies, waits for them, and re-layouts  23.1 us (7%)
  between operations  13.9 us (4%)
  other arithmetic  5.41 us (2%)
    all_to_all x1, blocking collectives, moved(): lax.all_to_all(group, axis, split_axis=split_dim, concat_axis=concat_dim,...  45.5 us
    pallas_call x2, Pallas kernels, flash(): pl.pallas_call(functools.partial(flash_body, d=d, dv=dv, nq=nq, nk=nk), o...  42.6 us
    ppermute x18, starting transfers between devices, ring(): return lambda a: lax.ppermute(a, axis, [(i, (i + t) % 4) for i in range(4)])  34.9 us
    all_to_all x1, waiting for transfers between devices, serve_rows(): lax.all_to_all(result.reshape(sources, items, width), SP_TP, split_axis=0...  30.1 us
    ppermute x18, waiting for transfers between devices, ring(): return lambda a: lax.ppermute(a, axis, [(i, (i + t) % 4) for i in range(4)])  17.9 us
    ppermute x6, waiting for transfers between devices, combine(): lax.ppermute(part[i * rows:(i + 1) * rows], 'z', [(j, (j - t) % 4) for j...  13.3 us
    ppermute x6, starting transfers between devices, combine(): lax.ppermute(part[i * rows:(i + 1) * rows], 'z', [(j, (j - t) % 4) for j...  11.7 us
    all_to_all x3, starting transfers between devices, moved_by_axis(): result = lax.all_to_all(result, axes[k], k, k, tiled=True)  11.3 us
  transfers between devices with their start and end apart: 32, of which 11 were waited for; matrix products, arithmetic and copies ran while one was open for 5% of the time, Pallas kernels for 17%

profile of v1, /device:TPU:1, one launch (start us, length us, event | category | flops | bytes accessed | tf_op | source)
XLA Modules:
  0.0 317.4 jit_solution(631157216750086456)
XLA Ops:
  14.6 6.9 %collective-permute-done.16 = bf16[384,256]{1,0:T(8,128)(2,1)S(1)} collective-permute-done((bf16[384,256]{1,0:T(8,128)(2,1)S(1)}, bf16[384,256]{1,0:T(8,128)(2,1)S(1)}, u32[]{:S(2)}, u32[]{:S(2)}) %collective-permute-start.16) | collective-permute-done | bytes 196640 | tf_op jit(solution)/shard_map/ppermute | solution.py:258
  35.8 5.9 %collective-permute-done.19.refs_7_ = bf16[768,256]{1,0:T(8,128)(2,1)S(1)} collective-permute-done((bf16[768,256]{1,0:T(8,128)(2,1)S(1)}, bf16[768,256]{1,0:T(8,128)(2,1)S(1)}, u32[]{:S(2)}, u32[]{:S(2)}) %collective-permute-start.19) | collective-permute-done | bytes 393248 | tf_op jit(solution)/shard_map/ppermute | solution.py:249
  41.7 19.8 %flash_narrow.1 = (f32[2,128,3072]{2,1,0:T(8,128)}, f32[4,3072]{1,0:T(4,128)S(1)}) custom-call(s32[12]{0:T(128)S(1)} %stack.51.pos_ref, bf16[768,128]{1,0:T(8,128)(2,1)S(1)} %bitcast.73, bf16[768,128]{1,0:T(8,128)(2,1)S(1)} %collective-permute-done.13.refs_1_, bf16[768,128]{1,0:T(8,128)(2,1)S(1)} %collective-permute-done.14.refs_2_, ...), custom_call_target="tpu_custom_call" | custom-call | flops 4303355904 | bytes 5505024 | tf_op jit(solution)/shard_map/flash_narrow/pallas_call | solution.py:189
  66.0 4.1 %collective-permute-start.5 = (bf16[768,512]{1,0:T(8,128)(2,1)S(1)}, bf16[768,512]{1,0:T(8,128)(2,1)S(1)}, u32[]{:S(2)}, u32[]{:S(2)}) collective-permute-start(bf16[768,512]{1,0:T(8,128)(2,1)S(1)} %pad_maximum_fusion.refs_4_), channel_id=1, source_target_pairs={{0,24},{8,0},{16,8},{24,16},{1,25},{9,1},{17,9},{25,17},{2,26},{10... | collective-permute-start | bytes 2359304 | tf_op jit(solution)/shard_map/ppermute | solution.py:249
  80.6 5.2 %mix_narrow.1 = bf16[3072,128]{1,0:T(8,128)(2,1)} custom-call(f32[2,1]{1,0:T(2,128)} %copy.71.lam_ref, f32[2,128,3072]{2,1,0:T(8,128)} %get-tuple-element.11.acc_ref, f32[4,3072]{1,0:T(4,128)} %copy-done, f32[4,3072]{1,0:T(4,128)} %copy-done.13, f32[4,3072]{1,0:T(4,128)} %copy-done.14, f32[4,3072]{1,0:T(4,128)} %copy-done.15), custom_call_target="tpu_custom_call" | custom-call | flops 1572864 | bytes 3932160 | tf_op jit(solution)/shard_map/mix_narrow/pallas_call | solution.py:236
  87.7 7.0 %collective-permute-start.24 = (bf16[768,128]{1,0:T(8,128)(2,1)S(1)}, bf16[768,128]{1,0:T(8,128)(2,1)S(1)}, u32[]{:S(2)}, u32[]{:S(2)}) collective-permute-start(bf16[768,128]{1,0:T(8,128)(2,1)S(1)} %get-tuple-element.18), channel_id=1, source_target_pairs={{0,32},{32,64},{64,96},{96,0},{1,33},{33,65},{65,97},{97,1},{2,34}... | collective-permute-start | bytes 589832 | tf_op jit(solution)/shard_map/ppermute | solution.py:285
  94.7 7.5 %collective-permute-done.6.refs_7_ = bf16[768,512]{1,0:T(8,128)(2,1)} collective-permute-done((bf16[768,512]{1,0:T(8,128)(2,1)S(1)}, bf16[768,512]{1,0:T(8,128)(2,1)}, u32[]{:S(2)}, u32[]{:S(2)}) %collective-permute-start.6) | collective-permute-done | bytes 786464 | tf_op jit(solution)/shard_map/ppermute | solution.py:249
  102.2 22.8 %flash_wide.1 = (f32[2,256,3072]{2,1,0:T(8,128)}, f32[4,3072]{1,0:T(4,128)S(1)}) custom-call(s32[12]{0:T(128)S(1)} %stack.51.pos_ref, bf16[768,256]{1,0:T(8,128)(2,1)S(1)} %bitcast.69, bf16[768,256]{1,0:T(8,128)(2,1)S(1)} %collective-permute-done.refs_1_, bf16[768,256]{1,0:T(8,128)(2,1)} %collective-permute-done.1.refs_2_, ...), custom_call_target="tpu_custom_call" | custom-call | flops 8606711808 | bytes 11010048 | tf_op jit(solution)/shard_map/flash_wide/pallas_call | solution.py:189
  125.1 3.6 %collective-permute-start.7 = (f32[4,3072]{1,0:T(4,128)S(1)}, f32[4,3072]{1,0:T(4,128)S(1)}, u32[]{:S(2)}, u32[]{:S(2)}) collective-permute-start(f32[4,3072]{1,0:T(4,128)S(1)} %get-tuple-element.32), channel_id=1, source_target_pairs={{0,32},{32,64},{64,96},{96,0},{1,33},{33,65},{65,97},{97,1},{2,34}... | collective-permute-start | bytes 147464 | tf_op jit(solution)/shard_map/ppermute | solution.py:249
  134.8 6.0 %mix_wide.1 = bf16[3072,256]{1,0:T(8,128)(2,1)} custom-call(f32[2,1]{1,0:T(2,128)} %copy.71.lam_ref, f32[2,256,3072]{2,1,0:T(8,128)} %get-tuple-element.9.acc_ref, f32[4,3072]{1,0:T(4,128)} %copy-done.1, f32[4,3072]{1,0:T(4,128)} %copy-done.16, f32[4,3072]{1,0:T(4,128)} %copy-done.17, f32[4,3072]{1,0:T(4,128)} %copy-done.18), custom_call_target="tpu_custom_call" | custom-call | flops 3145728 | bytes 7864320 | tf_op jit(solution)/shard_map/mix_wide/pallas_call | solution.py:236
  150.6 10.8 %collective-permute-done.11 = bf16[768,256]{1,0:T(8,128)(2,1)S(1)} collective-permute-done((bf16[768,256]{1,0:T(8,128)(2,1)S(1)}, bf16[768,256]{1,0:T(8,128)(2,1)S(1)}, u32[]{:S(2)}, u32[]{:S(2)}) %collective-permute-start.11) | collective-permute-done | bytes 393248 | tf_op jit(solution)/shard_map/ppermute | solution.py:285
  162.0 6.1 %all_to_all.30 = bf16[4,2,96,256]{3,2,0,1:T(8,128)(2,1)S(1)} all-to-all(bf16[4,2,96,256]{3,2,0,1:T(8,128)(2,1)S(1)} %copy.72), channel_id=1, replica_groups=mesh['z'=4,'x'=4,'y'=4,'c'=2] {'c'}, dimensions={1} | all-to-all | bytes 786432 | tf_op jit(solution)/shard_map/all_to_all | solution.py:323
  168.1 3.8 %all-to-all-start.2 = ((bf16[4,2,96,128]{3,2,0,1:T(8,128)(2,1)}), bf16[4,2,96,128]{3,2,0,1:T(8,128)(2,1)S(1)}, u32[]{:S(2)}, u32[]{:S(2)}) async-start(bf16[4,2,96,128]{3,2,0,1:T(8,128)(2,1)} %copy.76), calls=%async_computation.2 | async-start | bytes 393216 | tf_op jit(solution)/shard_map/all_to_all | solution.py:323
  173.0 4.2 %all-to-all-start.1 = ((bf16[4,2,96,256]{3,2,1,0:T(8,128)(2,1)}), bf16[4,2,96,256]{3,2,1,0:T(8,128)(2,1)S(1)}, u32[]{:S(2)}, u32[]{:S(2)}) async-start(bf16[4,2,96,256]{3,2,1,0:T(8,128)(2,1)} %copy.73), calls=%async_computation.1 | async-start | bytes 786432 | tf_op jit(solution)/shard_map/all_to_all | solution.py:323
  178.0 6.4 %all-to-all-done.1 = bf16[4,2,96,256]{3,2,1,0:T(8,128)(2,1)S(1)} async-done(((bf16[4,2,96,256]{3,2,1,0:T(8,128)(2,1)}), bf16[4,2,96,256]{3,2,1,0:T(8,128)(2,1)S(1)}, u32[]{:S(2)}, u32[]{:S(2)}) %all-to-all-start.1) | async-done | bytes 393248 | tf_op jit(solution)/shard_map/all_to_all | solution.py:323
  187.9 4.9 %fusion.34 = f32[96,2048]{1,0:T(8,128)S(1)} fusion(bf16[96,2048]{1,0:T(8,128)(2,1)S(1)} %bitcast.74, bf16[2048,2048]{1,0:T(8,128)(2,1)} %all-gather.3.cloned.1.call-done), kind=kOutput, calls=%fused_computation.67 | convolution fusion | flops 805306368 | bytes 9568256 | tf_op jit(solution)/shard_map/dot_general | solution.py:380
  198.0 4.0 %reshape.108 = bf16[128,3,2048]{2,1,0:T(4,128)(2,1)S(1)} reshape(bf16[384,2048]{1,0:T(8,128)(2,1)} %convolution_convert_fusion) | data formatting | bytes 3145728 | tf_op jit(solution)/shard_map/reshape | solution.py:405
  202.0 45.5 %all_to_all.31 = bf16[128,3,2048]{2,1,0:T(4,128)(2,1)} all-to-all(bf16[128,3,2048]{2,1,0:T(4,128)(2,1)S(1)} %reshape.108), channel_id=1, replica_groups=mesh['z'=4,'x'=4,'y'=4,'c'=2] {'z','x','y','c'}, dimensions={0} | all-to-all | bytes 3145728 | tf_op jit(solution)/shard_map/all_to_all | solution.py:335
  247.5 3.9 %reshape.109 = bf16[384,2048]{1,0:T(8,128)(2,1)S(1)} reshape(bf16[128,3,2048]{2,1,0:T(4,128)(2,1)} %all_to_all.31) | data formatting | bytes 3145728 | tf_op jit(solution)/shard_map/reshape | solution.py:409
  251.4 5.2 %fusion.4 = f32[384,1024]{1,0:T(8,128)} fusion(bf16[384,2048]{1,0:T(8,128)(2,1)S(1)} %reshape.109, bf16[1,2048,1024]{2,1,0:T(8,128)(2,1)} %param.29), kind=kOutput, calls=%fused_computation.4 | convolution fusion | flops 1610612736 | bytes 7340032 | tf_op jit(solution)/shard_map/dot_general | solution.py:410
  256.6 8.6 %fusion.6 = bf16[384,2048]{1,0:T(8,128)(2,1)} fusion(bf16[1,1024,2048]{2,1,0:T(8,128)(2,1)} %param.31, f32[384,1024]{1,0:T(8,128)} %fusion.4, bf16[384,2048]{1,0:T(8,128)(2,1)S(1)} %reshape.109, bf16[1,2048,1024]{2,1,0:T(8,128)(2,1)} %param.30), kind=kOutput, calls=%fused_computation.6 | convolution fusion | flops 3224371200 | bytes 13107200 | tf_op jit(solution)/shard_map/dot_general | solution.py:413
  265.2 5.2 %reshape.110 = bf16[128,3,2048]{2,1,0:T(4,128)(2,1)} reshape(bf16[384,2048]{1,0:T(8,128)(2,1)} %fusion.6) | data formatting | bytes 3145728 | tf_op jit(solution)/shard_map/reshape | solution.py:417
  270.3 4.9 %all-to-all-start.5 = ((bf16[128,3,2048]{2,1,0:T(4,128)(2,1)}), bf16[128,3,2048]{2,1,0:T(4,128)(2,1)S(1)}, u32[]{:S(2)}, u32[]{:S(2)}) async-start(bf16[128,3,2048]{2,1,0:T(4,128)(2,1)} %reshape.110), calls=%async_computation.5 | async-start | bytes 4194304 | tf_op jit(solution)/shard_map/all_to_all | solution.py:416
  275.3 30.1 %all-to-all-done.5 = bf16[128,3,2048]{2,1,0:T(4,128)(2,1)S(1)} async-done(((bf16[128,3,2048]{2,1,0:T(4,128)(2,1)}), bf16[128,3,2048]{2,1,0:T(4,128)(2,1)S(1)}, u32[]{:S(2)}, u32[]{:S(2)}) %all-to-all-start.5) | async-done | bytes 1572896 | tf_op jit(solution)/shard_map/all_to_all | solution.py:416
  (145 shorter events, 71.3 us)
Async XLA Ops:
  6.5 181.3 %all-gather.3.cloned.1.call-start = ((), (), s32[]{:S(2)}) async-start(), calls=%async_computation.6 | async-start | bytes 9437184 | tf_op jit(solution)/shard_map/all_gather | solution.py:373
  7.3 185.7 %all-gather.5.cloned.1.call-start = ((), (), s32[]{:S(2)}) async-start(), calls=%async_computation.7 | async-start | bytes 4718592 | tf_op jit(solution)/shard_map/all_gather | solution.py:374
  8.0 19.1 %collective-permute-start.13 = (bf16[768,128]{1,0:T(8,128)(2,1)S(1)}, bf16[768,128]{1,0:T(8,128)(2,1)S(1)}, u32[]{:S(2)}, u32[]{:S(2)}) collective-permute-start(bf16[768,128]{1,0:T(8,128)(2,1)S(1)} %bitcast.70), channel_id=1, source_target_pairs={{0,32},{32,64},{64,96},{96,0},{1,33},{33,65},{65,97},{97,1},{2,34}... | collective-permute-start | bytes 589832 | tf_op jit(solution)/shard_map/ppermute | solution.py:249
  10.6 17.9 %collective-permute-start.14 = (bf16[768,128]{1,0:T(8,128)(2,1)S(1)}, bf16[768,128]{1,0:T(8,128)(2,1)S(1)}, u32[]{:S(2)}, u32[]{:S(2)}) collective-permute-start(bf16[768,128]{1,0:T(8,128)(2,1)S(1)} %bitcast.71), channel_id=1, source_target_pairs={{0,96},{32,0},{64,32},{96,64},{1,97},{33,1},{65,33},{97,65},{2,98}... | collective-permute-start | bytes 589832 | tf_op jit(solution)/shard_map/ppermute | solution.py:249
  12.8 8.7 %collective-permute-start.16 = (bf16[384,256]{1,0:T(8,128)(2,1)S(1)}, bf16[384,256]{1,0:T(8,128)(2,1)S(1)}, u32[]{:S(2)}, u32[]{:S(2)}) collective-permute-start(bf16[384,256]{1,0:T(8,128)(2,1)S(1)} %get-tuple-element.22), channel_id=1, source_target_pairs={{0,96},{32,64},{64,32},{96,0},{1,97},{33,65},{65,33},{97,1},{2,98}... | collective-permute-start | bytes 589832 | tf_op jit(solution)/shard_map/ppermute | solution.py:258
  21.5 14.2 %collective-permute-start.17 = (bf16[768,256]{1,0:T(8,128)(2,1)S(1)}, bf16[768,256]{1,0:T(8,128)(2,1)S(1)}, u32[]{:S(2)}, u32[]{:S(2)}) collective-permute-start(bf16[768,256]{1,0:T(8,128)(2,1)S(1)} %pad_maximum_fusion.2.refs_4_), channel_id=1, source_target_pairs={{0,8},{8,16},{16,24},{24,0},{1,9},{9,17},{17,25},{25,1},{2,10},{10... | collective-permute-start | bytes 1179656 | tf_op jit(solution)/shard_map/ppermute | solution.py:249
  22.8 12.9 %collective-permute-start.18 = (bf16[768,256]{1,0:T(8,128)(2,1)S(1)}, bf16[768,256]{1,0:T(8,128)(2,1)S(1)}, u32[]{:S(2)}, u32[]{:S(2)}) collective-permute-start(bf16[768,256]{1,0:T(8,128)(2,1)S(1)} %pad_maximum_fusion.2.refs_4_), channel_id=1, source_target_pairs={{0,24},{8,0},{16,8},{24,16},{1,25},{9,1},{17,9},{25,17},{2,26},{10... | collective-permute-start | bytes 1179656 | tf_op jit(solution)/shard_map/ppermute | solution.py:249
  24.3 17.4 %collective-permute-start.19 = (bf16[768,256]{1,0:T(8,128)(2,1)S(1)}, bf16[768,256]{1,0:T(8,128)(2,1)S(1)}, u32[]{:S(2)}, u32[]{:S(2)}) collective-permute-start(bf16[768,256]{1,0:T(8,128)(2,1)S(1)} %pad_maximum_fusion.2.refs_4_), channel_id=1, source_target_pairs={{0,16},{8,24},{16,0},{24,8},{1,17},{9,25},{17,1},{25,9},{2,18},{10... | collective-permute-start | bytes 1179656 | tf_op jit(solution)/shard_map/ppermute | solution.py:249
  28.4 43.8 %collective-permute-start = (bf16[768,256]{1,0:T(8,128)(2,1)S(1)}, bf16[768,256]{1,0:T(8,128)(2,1)S(1)}, u32[]{:S(2)}, u32[]{:S(2)}) collective-permute-start(bf16[768,256]{1,0:T(8,128)(2,1)S(1)} %bitcast.66), channel_id=1, source_target_pairs={{0,32},{32,64},{64,96},{96,0},{1,33},{33,65},{65,97},{97,1},{2,34}... | collective-permute-start | bytes 1179656 | tf_op jit(solution)/shard_map/ppermute | solution.py:249
  33.3 31.1 %collective-permute-start.3 = (bf16[384,512]{1,0:T(8,128)(2,1)S(1)}, bf16[384,512]{1,0:T(8,128)(2,1)S(1)}, u32[]{:S(2)}, u32[]{:S(2)}) collective-permute-start(bf16[384,512]{1,0:T(8,128)(2,1)S(1)} %get-tuple-element.20), channel_id=1, source_target_pairs={{0,96},{32,64},{64,32},{96,0},{1,97},{33,65},{65,33},{97,1},{2,98}... | collective-permute-start | bytes 1179656 | tf_op jit(solution)/shard_map/ppermute | solution.py:258
  62.1 11.2 %collective-permute-start.20 = (f32[4,3072]{1,0:T(4,128)S(1)}, f32[4,3072]{1,0:T(4,128)S(1)}, u32[]{:S(2)}, u32[]{:S(2)}) collective-permute-start(f32[4,3072]{1,0:T(4,128)S(1)} %get-tuple-element.25), channel_id=1, source_target_pairs={{0,32},{32,64},{64,96},{96,0},{1,33},{33,65},{65,97},{97,1},{2,34}... | collective-permute-start | bytes 147464 | tf_op jit(solution)/shard_map/ppermute | solution.py:249
  64.5 30.2 %collective-permute-start.4 = (bf16[768,512]{1,0:T(8,128)(2,1)S(1)}, bf16[768,512]{1,0:T(8,128)(2,1)S(1)}, u32[]{:S(2)}, u32[]{:S(2)}) collective-permute-start(bf16[768,512]{1,0:T(8,128)(2,1)S(1)} %pad_maximum_fusion.refs_4_), channel_id=1, source_target_pairs={{0,8},{8,16},{16,24},{24,0},{1,9},{9,17},{17,25},{25,1},{2,10},{10... | collective-permute-start | bytes 2359304 | tf_op jit(solution)/shard_map/ppermute | solution.py:249
  66.0 28.8 %collective-permute-start.5 = (bf16[768,512]{1,0:T(8,128)(2,1)S(1)}, bf16[768,512]{1,0:T(8,128)(2,1)S(1)}, u32[]{:S(2)}, u32[]{:S(2)}) collective-permute-start(bf16[768,512]{1,0:T(8,128)(2,1)S(1)} %pad_maximum_fusion.refs_4_), channel_id=1, source_target_pairs={{0,24},{8,0},{16,8},{24,16},{1,25},{9,1},{17,9},{25,17},{2,26},{10... | collective-permute-start | bytes 2359304 | tf_op jit(solution)/shard_map/ppermute | solution.py:249
  70.0 32.2 %collective-permute-start.6 = (bf16[768,512]{1,0:T(8,128)(2,1)S(1)}, bf16[768,512]{1,0:T(8,128)(2,1)}, u32[]{:S(2)}, u32[]{:S(2)}) collective-permute-start(bf16[768,512]{1,0:T(8,128)(2,1)S(1)} %pad_maximum_fusion.refs_4_), channel_id=1, source_target_pairs={{0,16},{8,24},{16,0},{24,8},{1,17},{9,25},{17,1},{25,9},{2,18},{10... | collective-permute-start | bytes 2359304 | tf_op jit(solution)/shard_map/ppermute | solution.py:249
  76.9 10.1 %collective-permute-start.1 = (bf16[768,256]{1,0:T(8,128)(2,1)S(1)}, bf16[768,256]{1,0:T(8,128)(2,1)}, u32[]{:S(2)}, u32[]{:S(2)}) collective-permute-start(bf16[768,256]{1,0:T(8,128)(2,1)S(1)} %bitcast.67), channel_id=1, source_target_pairs={{0,96},{32,0},{64,32},{96,64},{1,97},{33,1},{65,33},{97,65},{2,98}... | collective-permute-start | bytes 1179656 | tf_op jit(solution)/shard_map/ppermute | solution.py:249
  77.2 10.5 %collective-permute-start.2 = (bf16[768,256]{1,0:T(8,128)(2,1)S(1)}, bf16[768,256]{1,0:T(8,128)(2,1)}, u32[]{:S(2)}, u32[]{:S(2)}) collective-permute-start(bf16[768,256]{1,0:T(8,128)(2,1)S(1)} %bitcast.68), channel_id=1, source_target_pairs={{0,64},{32,96},{64,0},{96,32},{1,65},{33,97},{65,1},{97,33},{2,66}... | collective-permute-start | bytes 1179656 | tf_op jit(solution)/shard_map/ppermute | solution.py:249
  87.0 43.2 %collective-permute-start.25 = (bf16[768,128]{1,0:T(8,128)(2,1)S(1)}, bf16[768,128]{1,0:T(8,128)(2,1)S(1)}, u32[]{:S(2)}, u32[]{:S(2)}) collective-permute-start(bf16[768,128]{1,0:T(8,128)(2,1)S(1)} %get-tuple-element.17), channel_id=1, source_target_pairs={{0,64},{32,96},{64,0},{96,32},{1,65},{33,97},{65,1},{97,33},{2,66}... | collective-permute-start | bytes 589832 | tf_op jit(solution)/shard_map/ppermute | solution.py:285
  87.7 44.5 %collective-permute-start.24 = (bf16[768,128]{1,0:T(8,128)(2,1)S(1)}, bf16[768,128]{1,0:T(8,128)(2,1)S(1)}, u32[]{:S(2)}, u32[]{:S(2)}) collective-permute-start(bf16[768,128]{1,0:T(8,128)(2,1)S(1)} %get-tuple-element.18), channel_id=1, source_target_pairs={{0,32},{32,64},{64,96},{96,0},{1,33},{33,65},{65,97},{97,1},{2,34}... | collective-permute-start | bytes 589832 | tf_op jit(solution)/shard_map/ppermute | solution.py:285
  94.7 37.5 %collective-permute-start.23 = (bf16[768,128]{1,0:T(8,128)(2,1)S(1)}, bf16[768,128]{1,0:T(8,128)(2,1)S(1)}, u32[]{:S(2)}, u32[]{:S(2)}) collective-permute-start(bf16[768,128]{1,0:T(8,128)(2,1)S(1)} %get-tuple-element.16), channel_id=1, source_target_pairs={{0,96},{32,0},{64,32},{96,64},{1,97},{33,1},{65,33},{97,65},{2,98}... | collective-permute-start | bytes 589832 | tf_op jit(solution)/shard_map/ppermute | solution.py:285
  125.1 9.0 %collective-permute-start.7 = (f32[4,3072]{1,0:T(4,128)S(1)}, f32[4,3072]{1,0:T(4,128)S(1)}, u32[]{:S(2)}, u32[]{:S(2)}) collective-permute-start(f32[4,3072]{1,0:T(4,128)S(1)} %get-tuple-element.32), channel_id=1, source_target_pairs={{0,32},{32,64},{64,96},{96,0},{1,33},{33,65},{65,97},{97,1},{2,34}... | collective-permute-start | bytes 147464 | tf_op jit(solution)/shard_map/ppermute | solution.py:249
  143.6 17.8 %collective-permute-start.11 = (bf16[768,256]{1,0:T(8,128)(2,1)S(1)}, bf16[768,256]{1,0:T(8,128)(2,1)S(1)}, u32[]{:S(2)}, u32[]{:S(2)}) collective-permute-start(bf16[768,256]{1,0:T(8,128)(2,1)S(1)} %get-tuple-element.15), channel_id=1, source_target_pairs={{0,32},{32,64},{64,96},{96,0},{1,33},{33,65},{65,97},{97,1},{2,34}... | collective-permute-start | bytes 1179656 | tf_op jit(solution)/shard_map/ppermute | solution.py:285
  145.2 16.2 %collective-permute-start.10 = (bf16[768,256]{1,0:T(8,128)(2,1)S(1)}, bf16[768,256]{1,0:T(8,128)(2,1)S(1)}, u32[]{:S(2)}, u32[]{:S(2)}) collective-permute-start(bf16[768,256]{1,0:T(8,128)(2,1)S(1)} %get-tuple-element.13), channel_id=1, source_target_pairs={{0,96},{32,0},{64,32},{96,64},{1,97},{33,1},{65,33},{97,65},{2,98}... | collective-permute-start | bytes 1179656 | tf_op jit(solution)/shard_map/ppermute | solution.py:285
  173.0 11.4 %all-to-all-start.1 = ((bf16[4,2,96,256]{3,2,1,0:T(8,128)(2,1)}), bf16[4,2,96,256]{3,2,1,0:T(8,128)(2,1)S(1)}, u32[]{:S(2)}, u32[]{:S(2)}) async-start(bf16[4,2,96,256]{3,2,1,0:T(8,128)(2,1)} %copy.73), calls=%async_computation.1 | async-start | bytes 786432 | tf_op jit(solution)/shard_map/all_to_all | solution.py:323
  270.3 35.1 %all-to-all-start.5 = ((bf16[128,3,2048]{2,1,0:T(4,128)(2,1)}), bf16[128,3,2048]{2,1,0:T(4,128)(2,1)S(1)}, u32[]{:S(2)}, u32[]{:S(2)}) async-start(bf16[128,3,2048]{2,1,0:T(4,128)(2,1)} %reshape.110), calls=%async_computation.5 | async-start | bytes 4194304 | tf_op jit(solution)/shard_map/all_to_all | solution.py:416
  (31 other events, 207.5 us)
Sparse Core Ops, SparseCore 0:
  9.1 53.2 all-gather.2
  64.1 32.2 all-gather.4

commit v2 on v0

v2 whole, which is shorter than its diff:
```python
import functools
import jax
import jax.numpy as jnp
from jax import lax
from jax.experimental import pallas as pl
from jax.experimental.pallas import tpu as pltpu
from jax.sharding import Mesh
from jax.sharding import PartitionSpec as P

TP = ("y", "c")
SP = ("z", "x")
SP_TP = ("z", "x", "y", "c")

NEG = -1e30
LOG2E = 1.4426950408889634
TQ = 256
CH = 256
SHIFTS = (0, 1, 3, 2)
SLOT = {t: i for i, t in enumerate(SHIFTS)}


class Copies:
    def __init__(self, send_sems, recv_sems):
        self.send_sems, self.recv_sems, self.all = send_sems, recv_sems, []

    def make(self, src, dst, **device):
        n = len(self.all)
        copy = pltpu.make_async_remote_copy(
            src_ref=src,
            dst_ref=dst,
            send_sem=self.send_sems.at[n],
            recv_sem=self.recv_sems.at[n],
            device_id=device,
            device_id_type=pl.DeviceIdType.MESH,
        )
        self.all.append(copy)
        return copy


class Heads:
    def __init__(self, d, dv, rows, ins, refs, shared, copies):
        self.d, self.dv, self.rows, self.half = d, dv, rows, rows // 2
        self.q_in, self.kv_in = ins
        self.q_s, self.kv_s, self.qt_s, self.vt_s, self.acc, self.st, self.st_in, self.part, self.part_in, self.relay, self.heads, self.out = refs
        self.tab, self.pos, self.s_a, self.s_b, self.t_a, self.t_b, self.p_scr, self.m_s, self.l_s = shared
        self.scale = d ** (-0.5) * LOG2E
        self.copies = copies
        z, x = lax.axis_index("z"), lax.axis_index("x")
        up = {"z": (z + 1) % 4}, {"z": (z + 3) % 4}
        right = {"x": (x + 1) % 4}, {"x": (x + 3) % 4}
        half = self.half
        one, three, two = SLOT[1], SLOT[3], SLOT[2]
        h0, h1 = pl.ds(0, half), pl.ds(half, half)
        self.q_near = [copies.make(self.q_in, self.q_s.at[one], **up[0]), copies.make(self.q_in, self.q_s.at[three], **up[1])]
        self.q_far = [
            copies.make(self.q_s.at[one, h0], self.q_s.at[two, h0], **up[0]),
            copies.make(self.q_s.at[three, h1], self.q_s.at[two, h1], **up[1]),
        ]
        self.swap = copies.make(self.kv_in.at[h1], self.kv_s.at[1, 0], z=3 - z)
        self.kv_near, self.kv_far = [], []
        quarter = half // 2
        g0, g1 = pl.ds(0, quarter), pl.ds(quarter, quarter)
        for b in range(2):
            src = self.kv_in.at[h0] if b == 0 else self.kv_s.at[1, 0]
            self.kv_near.append([copies.make(src, self.kv_s.at[b, one], **right[0]), copies.make(src, self.kv_s.at[b, three], **right[1])])
            self.kv_far.append([
                copies.make(self.kv_s.at[b, one, g0], self.kv_s.at[b, two, g0], **right[0]),
                copies.make(self.kv_s.at[b, three, g1], self.kv_s.at[b, two, g1], **right[1]),
            ])
        self.st_out = [copies.make(self.st, self.st_in.at[t - 1], z=(z + t) % 4) for t in (1, 2, 3)]
        self.part_near = [
            copies.make(self.part.at[one], self.part_in.at[0], **up[1]),
            copies.make(self.part.at[three], self.part_in.at[1], **up[0]),
        ]
        self.part_first = [
            copies.make(self.part.at[two, h0], self.relay.at[0], **up[0]),
            copies.make(self.part.at[two, h1], self.relay.at[1], **up[1]),
        ]
        self.part_far = [
            copies.make(self.relay.at[0], self.part_in.at[2, h0], **up[0]),
            copies.make(self.relay.at[1], self.part_in.at[2, h1], **up[1]),
        ]
        rank = lax.axis_index("y") * 2 + lax.axis_index("c")
        self.rank = rank
        mine = rows // 8
        self.to_tokens = []
        for k in range(1, 8):
            r = (rank + k) % 8
            self.to_tokens.append(copies.make(
                self.heads.at[pl.ds(pl.multiple_of(r * mine, mine), mine)],
                self.out.at[:, pl.ds(pl.multiple_of(rank * dv, dv), dv)],
                y=r // 2, c=r % 2,
            ))

    def send_swap(self):
        self.swap.start()

    def send_near(self):
        for c in self.kv_near[0] + self.q_near:
            c.start()

    def pass_swap(self):
        self.swap.wait_recv()
        for c in self.kv_near[1]:
            c.start()

    def relay_first(self):
        for near, far in zip(self.kv_near[0] + self.q_near, self.kv_far[0] + self.q_far):
            near.wait_recv()
            far.start()

    def relay_second(self):
        for near, far in zip(self.kv_near[1], self.kv_far[1]):
            near.wait_recv()
            far.start()

    def wait_all(self):
        for c in self.kv_far[0] + self.kv_far[1] + self.q_far:
            c.wait_recv()

    def prepare(self):
        d, dv, rows, half = self.d, self.dv, self.rows, self.half

        def turn(i, _):
            r = pl.multiple_of(i * rows, rows)
            self.qt_s[:, pl.ds(r, rows)] = self.q_s[i].T
            return 0
        lax.fori_loop(0, 4, turn, 0)

        def turn_v(i, _):
            r = pl.multiple_of(i * half, half)
            self.vt_s[:, pl.ds(r, half)] = self.kv_s[i // 4, i % 4, :, 2 * d:2 * d + dv].T
            return 0
        lax.fori_loop(0, 8, turn_v, 0)

    def read(self, i, s_buf, t_buf):
        d, half = self.d, self.half
        q0 = pl.multiple_of(self.tab[0, i] * TQ, TQ)
        kj = self.tab[1, i]
        part, first = kj // 2, (kj % 2) * 2
        for w in range(2):
            qt = self.qt_s[w * d:(w + 1) * d, pl.ds(q0, TQ)]
            top = None
            for c in range(2):
                k = self.kv_s[part, first + c, :, w * d:(w + 1) * d]
                s = jnp.dot(k, qt, preferred_element_type=jnp.float32)
                s_buf[w, c * half:(c + 1) * half] = s
                m8 = jnp.max(s.reshape(half // 8, 8, TQ), axis=0)
                top = m8 if top is None else jnp.maximum(top, m8)
            t_buf[w] = top

    def mask(self, i, s_buf, t_buf):
        rows, half = self.rows, self.half
        per = rows // TQ
        qi, kj = self.tab[0, i], self.tab[1, i]
        qp = self.pos[qi // per] + (qi % per) * TQ
        CM = 128
        t_buf[...] = jnp.full_like(t_buf, NEG)

        def chunk(c, _):
            r = pl.multiple_of(c * CM, CM)
            late = c // (half // CM)
            k0 = self.pos[4 + 2 * kj + late] + (c - late * (half // CM)) * CM
            keep = lax.broadcasted_iota(jnp.int32, (CM, TQ), 0) - lax.broadcasted_iota(jnp.int32, (CM, TQ), 1) <= qp - k0
            for w in range(2):
                s = jnp.where(keep, s_buf[w, pl.ds(r, CM)], NEG)
                s_buf[w, pl.ds(r, CM)] = s
                t_buf[w] = jnp.maximum(t_buf[w], jnp.max(s.reshape(CM // 8, 8, TQ), axis=0))
            return 0
        lax.fori_loop(0, rows // CM, chunk, 0)

    def weigh(self, i, q0, s_buf, t_buf):
        rows = self.rows
        k0 = pl.multiple_of(self.tab[1, i] * rows, rows)
        for w in range(2):
            old = self.m_s[w:w + 1]
            new = jnp.maximum(old, jnp.max(t_buf[w], axis=0, keepdims=True) * self.scale)
            f = jnp.exp2(old - new)
            self.m_s[w:w + 1] = new
            tot = None
            for c in range(rows // CH):
                p = jnp.exp2(s_buf[w, c * CH:(c + 1) * CH] * self.scale - new)
                t8 = jnp.sum(p.reshape(CH // 8, 8, TQ), axis=0)
                tot = t8 if tot is None else tot + t8
                self.p_scr[w, c * CH:(c + 1) * CH] = p.astype(jnp.bfloat16)
            o = jnp.dot(self.vt_s[:, pl.ds(k0, rows)], self.p_scr[w], preferred_element_type=jnp.float32)
            self.l_s[w] = self.l_s[w] * f + tot
            self.acc[w, :, pl.ds(q0, TQ)] = self.acc[w, :, pl.ds(q0, TQ)] * f + o

    def run(self, steps, hooks):
        def advance(i, cur, nxt):
            q0 = pl.multiple_of(self.tab[0, i] * TQ, TQ)

            @pl.when(self.tab[3, i] == 1)
            def _():
                self.m_s[...] = jnp.full_like(self.m_s, NEG)
                self.l_s[...] = jnp.zeros_like(self.l_s)
                self.acc[:, :, pl.ds(q0, TQ)] = jnp.zeros((2, self.dv, TQ), jnp.float32)

            @pl.when(self.tab[2, i] == 1)
            def _():
                self.mask(i, *cur)
            self.read(jnp.minimum(i + 1, steps - 1), *nxt)
            self.weigh(i, q0, *cur)

            @pl.when(self.tab[3, i + 1] == 1)
            def _():
                self.st[0:2, pl.ds(q0, TQ)] = self.m_s[...]
                for w in range(2):
                    self.st[2 + w:3 + w, pl.ds(q0, TQ)] = jnp.sum(self.l_s[w], axis=0, keepdims=True)

        one, two = (self.s_a, self.t_a), (self.s_b, self.t_b)
        self.read(0, *one)
        pairs = (steps + 1) // 2

        def pair(n, _):
            for k, hook in enumerate(hooks):
                pl.when(n == pairs * (k + 1) // (len(hooks) + 1))(hook)
            advance(2 * n, one, two)

            @pl.when(2 * n + 1 < steps)
            def _():
                advance(2 * n + 1, two, one)
            return 0
        lax.fori_loop(0, pairs, pair, 0)

    def mix(self, slot, lam):
        rows, dv = self.rows, self.dv
        for p in range(rows // TQ):
            c0 = slot * rows + p * TQ
            stats = [self.st[:, c0:c0 + TQ]]
            for t in (1, 2, 3):
                at = SLOT[(SHIFTS[slot] - t) % 4] * rows + p * TQ
                stats.append(self.st_in[t - 1, :, at:at + TQ])
            weights = []
            for w in range(2):
                peaks = [s[w:w + 1] for s in stats]
                top = functools.reduce(jnp.maximum, peaks)
                total = sum(s[2 + w:3 + w] * jnp.exp2(m - top) for m, s in zip(peaks, stats))
                weights.append(jnp.exp2(peaks[0] - top) / total)
            mixed = self.acc[0, :, c0:c0 + TQ] * weights[0] - self.acc[1, :, c0:c0 + TQ] * (weights[1] * lam)
            self.part[slot, p * TQ:(p + 1) * TQ] = mixed.T.astype(jnp.bfloat16)

    def send_stats(self):
        for c in self.st_out:
            c.start()

    def mix_and_send(self, lam):
        for c in self.st_out:
            c.wait_recv()
        self.mix(SLOT[2], lam)
        for c in self.part_first:
            c.start()
        self.mix(SLOT[1], lam)
        self.part_near[0].start()
        self.mix(SLOT[3], lam)
        self.part_near[1].start()

    def pass_parts(self):
        for first, far in zip(self.part_first, self.part_far):
            first.wait_recv()
            far.start()

    def finish(self):
        for c in self.part_near + self.part_far:
            c.wait_recv()
        B = 192
        for p in range(self.rows // B):
            r = slice(p * B, (p + 1) * B)
            total = self.part[0, r].astype(jnp.float32)
            for n in range(3):
                total = total + self.part_in[n, r].astype(jnp.float32)
            total = total * lax.rsqrt(jnp.mean(total * total, axis=-1, keepdims=True) + 1e-06)
            self.heads[r] = total.astype(jnp.bfloat16)
        for c in self.to_tokens:
            c.start()
        mine = self.rows // 8
        at = pl.multiple_of(self.rank * mine, mine)
        self.out[:, pl.ds(pl.multiple_of(self.rank * self.dv, self.dv), self.dv)] = self.heads[pl.ds(at, mine)]


def attention_kernel(lam_ref, qn_in, kvn_in, qw_in, kvw_in, out_w, out_n, *scratch, rows):
    narrow_refs, wide_refs = scratch[:12], scratch[12:24]
    shared, (send_sems, recv_sems, local_sems) = scratch[24:33], scratch[33:36]
    z, x = lax.axis_index("z"), lax.axis_index("x")
    half = rows // 2
    copies = Copies(send_sems, recv_sems)
    narrow = Heads(64, 128, rows, (qn_in, kvn_in), narrow_refs, shared, copies)
    wide = Heads(128, 256, rows, (qw_in, kvw_in), wide_refs, shared, copies)

    barrier = pltpu.get_barrier_semaphore()
    for t in (1, 2, 3):
        pl.semaphore_signal(barrier, inc=1, device_id={"z": (z + t) % 4}, device_id_type=pl.DeviceIdType.MESH)
        pl.semaphore_signal(barrier, inc=1, device_id={"x": (x + t) % 4}, device_id_type=pl.DeviceIdType.MESH)
    rank = narrow.rank
    for k in range(1, 8):
        r = (rank + k) % 8
        pl.semaphore_signal(barrier, inc=1, device_id={"y": r // 2, "c": r % 2}, device_id_type=pl.DeviceIdType.MESH)
    local = []
    for h in (narrow, wide):
        local.append(pltpu.make_async_copy(h.q_in, h.q_s.at[0], local_sems.at[len(local)]))
        local.append(pltpu.make_async_copy(h.kv_in.at[pl.ds(0, half)], h.kv_s.at[0, 0], local_sems.at[len(local)]))
    for c in local:
        c.start()
    pl.semaphore_wait(barrier, 13)

    narrow.send_swap()
    narrow.send_near()
    wide.send_swap()
    narrow.pass_swap()
    wide.send_near()

    pos, tab = narrow.pos, narrow.tab
    for i, t in enumerate(SHIFTS):
        pos[i] = (4 * ((z + 4 - t) % 4) + x) * rows
        n = (x + 4 - t) % 4
        pos[4 + i] = (4 * z + n) * rows
        pos[8 + i] = (4 * (3 - z) + n) * rows + half
    per = rows // TQ

    def list_q(qi, n):
        qp = pos[qi // per] + (qi % per) * TQ

        def list_k(kj, carry):
            n, first = carry
            p0, p1 = pos[4 + 2 * kj], pos[4 + 2 * kj + 1]
            hi, lo = jnp.maximum(p0, p1), jnp.minimum(p0, p1)
            full = hi + half - 1 <= qp
            some = lo <= qp + TQ - 1
            tab[0, n] = qi
            tab[1, n] = kj
            tab[2, n] = jnp.where(full, 0, 1)
            tab[3, n] = first
            return n + jnp.where(some, 1, 0), jnp.where(some, 0, first)
        m, _ = lax.fori_loop(0, 4, list_k, (n, 1))

        @pl.when(m == n)
        def _():
            tab[0, n] = qi
            tab[1, n] = 0
            tab[2, n] = 1
            tab[3, n] = 1
        return jnp.maximum(m, n + 1)
    steps = lax.fori_loop(0, 4 * per, list_q, 0)
    tab[3, steps] = 1

    narrow.relay_first()
    narrow.relay_second()
    wide.pass_swap()
    narrow.wait_all()
    for c in local:
        c.wait()
    narrow.prepare()
    narrow.run(steps, [wide.relay_first, wide.relay_second])
    narrow.send_stats()
    wide.wait_all()
    wide.prepare()
    narrow.mix_and_send(lam_ref[1, 0])
    narrow.mix(0, lam_ref[1, 0])
    wide.run(steps, [narrow.pass_parts, narrow.finish])
    wide.send_stats()
    wide.mix_and_send(lam_ref[0, 0])
    wide.pass_parts()
    wide.mix(0, lam_ref[0, 0])
    wide.finish()
    for h in (narrow, wide):
        for c in h.to_tokens:
            c.wait_recv()
    out_n[...] = narrow.out[...]
    out_w[...] = wide.out[...]
    for c in copies.all:
        c.wait_send()


def attention(qw, kw, vw, qn, kn, vn, lam):
    qw, kw, vw, qn, kn, vn = (a[:, 0] for a in (qw, kw, vw, qn, kn, vn))
    rows = qw.shape[0]
    half, mine = rows // 2, rows // 8

    def scratch(d, dv):
        return [
            pltpu.VMEM((4, rows, 2 * d), jnp.bfloat16),
            pltpu.VMEM((2, 4, half, 2 * d + dv), jnp.bfloat16),
            pltpu.VMEM((2 * d, 4 * rows), jnp.bfloat16),
            pltpu.VMEM((dv, 4 * rows), jnp.bfloat16),
            pltpu.VMEM((2, dv, 4 * rows), jnp.float32),
            pltpu.VMEM((4, 4 * rows), jnp.float32),
            pltpu.VMEM((3, 4, 4 * rows), jnp.float32),
            pltpu.VMEM((4, rows, dv), jnp.bfloat16),
            pltpu.VMEM((3, rows, dv), jnp.bfloat16),
            pltpu.VMEM((2, half, dv), jnp.bfloat16),
            pltpu.VMEM((rows, dv), jnp.bfloat16),
            pltpu.VMEM((mine, 8 * dv), jnp.bfloat16),
        ]
    any_ = pl.BlockSpec(memory_space=pl.ANY)
    vmem = pl.BlockSpec(memory_space=pltpu.VMEM)
    count = 2 * (2 + 2 + 1 + 8 + 3 + 6 + 7)
    return pl.pallas_call(
        functools.partial(attention_kernel, rows=rows),
        out_shape=(jax.ShapeDtypeStruct((mine, 8 * 256), jnp.bfloat16), jax.ShapeDtypeStruct((mine, 8 * 128), jnp.bfloat16)),
        in_specs=[pl.BlockSpec(memory_space=pltpu.SMEM)] + [any_] * 4,
        out_specs=(vmem, vmem),
        scratch_shapes=scratch(64, 128) + scratch(128, 256) + [
            pltpu.SMEM((4, 4 * (rows // TQ) * 4 + 1), jnp.int32),
            pltpu.SMEM((12,), jnp.int32),
            pltpu.VMEM((2, rows, TQ), jnp.float32),
            pltpu.VMEM((2, rows, TQ), jnp.float32),
            pltpu.VMEM((2, 8, TQ), jnp.float32),
            pltpu.VMEM((2, 8, TQ), jnp.float32),
            pltpu.VMEM((2, rows, TQ), jnp.bfloat16),
            pltpu.VMEM((2, TQ), jnp.float32),
            pltpu.VMEM((2, 8, TQ), jnp.float32),
            pltpu.SemaphoreType.DMA((count,)),
            pltpu.SemaphoreType.DMA((count,)),
            pltpu.SemaphoreType.DMA((4,)),
        ],
        name="attention",
        cost_estimate=pl.CostEstimate(flops=100 * 10**9, bytes_accessed=10**7, transcendentals=0),
        compiler_params=pltpu.CompilerParams(collective_id=0, has_side_effects=True, vmem_limit_bytes=60 * 2**20),
    )(lam, qn, jnp.concatenate([kn, vn], axis=1), qw, jnp.concatenate([kw, vw], axis=1))


def exchange_in_groups(array, axis, split_dim, concat_dim, work, item_dim, out_dim):

    def moved(group):
        return lax.all_to_all(group, axis, split_axis=split_dim, concat_axis=concat_dim, tiled=True)

    items = jax.tree.leaves(array)[0].shape[item_dim]
    ends = [items * k // 2 for k in range(2 + 1)] if items % 2 == 0 else [0, items]
    groups = [
        jax.tree.map(lambda a: lax.slice_in_dim(a, low, high, axis=item_dim), array)
        for low, high in zip(ends, ends[1:])
    ]
    arrived = [moved(group) for group in groups]
    made = [work(group) for group in arrived]
    return jax.tree.map(lambda *parts: jnp.concatenate(parts, axis=out_dim), *made)


def shards(
    query_wide,
    key_wide,
    value_wide,
    query_narrow,
    key_narrow,
    value_narrow,
    mix_lambda,
    residual_in,
    out_wide,
    out_narrow,
    ffn_gain,
    expert_ids,
    expert_weights,
    gate_weight,
    up_weight,
    down_weight,
):
    tok_count, local_heads, _ = query_wide.shape
    mine_wide, mine_narrow = attention(
        query_wide, key_wide, value_wide, query_narrow, key_narrow, value_narrow, mix_lambda
    )
    tp_size = lax.axis_size(TP)
    local_rows = tok_count // tp_size
    whole_wide, whole_narrow = (
        lax.all_gather(out_wide, TP, axis=0, tiled=True),
        lax.all_gather(out_narrow, TP, axis=0, tiled=True),
    )
    projected = jnp.dot(mine_wide, whole_wide, preferred_element_type=jnp.float32) + jnp.dot(
        mine_narrow, whole_narrow, preferred_element_type=jnp.float32
    )
    stream = (projected + residual_in.astype(jnp.float32)).astype(jnp.bfloat16)
    stream_f = stream.astype(jnp.float32)
    normed = (
        stream_f
        * lax.rsqrt(jnp.mean(stream_f * stream_f, axis=-1, keepdims=True) + 1e-06)
        * ffn_gain
    ).astype(jnp.bfloat16)
    experts_all = lax.axis_size(SP) * tp_size
    capacity = max(2, 4 * local_rows // experts_all)
    model_width = normed.shape[1]
    flat_expert = expert_ids.reshape(-1)
    expert_hot = (flat_expert[:, None] == jnp.arange(experts_all, dtype=jnp.int32)[None, :]).astype(
        jnp.int32
    )
    slot_rank = jnp.sum((jnp.cumsum(expert_hot, axis=0) - 1) * expert_hot, axis=1)
    flat_slot = flat_expert * capacity + slot_rank
    slot_ids = jnp.arange(experts_all * capacity, dtype=jnp.int32)
    placed = slot_ids[:, None] == flat_slot[None, :]
    dispatch = jnp.any(placed.reshape(experts_all * capacity, local_rows, 2), axis=2).astype(
        jnp.bfloat16
    )
    outgoing = jnp.dot(dispatch, normed, preferred_element_type=jnp.float32).astype(jnp.bfloat16)
    outgoing = outgoing.reshape(experts_all, capacity, model_width)

    def serve_rows(arrived):
        sources, items, width = arrived.shape
        flat_rows = arrived.reshape(sources * items, width)
        gate_part = jnp.dot(flat_rows, gate_weight[0], preferred_element_type=jnp.float32)
        up_part = jnp.dot(flat_rows, up_weight[0], preferred_element_type=jnp.float32)
        hidden = (jax.nn.silu(gate_part) * up_part).astype(jnp.bfloat16)
        result = jnp.dot(hidden, down_weight[0], preferred_element_type=jnp.float32).astype(
            jnp.bfloat16
        )
        return lax.all_to_all(
            result.reshape(sources, items, width), SP_TP, split_axis=0, concat_axis=0, tiled=True
        )

    returned = exchange_in_groups(outgoing, SP_TP, 0, 0, serve_rows, 1, 1)
    slot_hot = (flat_slot[:, None] == slot_ids[None, :]).astype(
        jnp.float32
    ) * expert_weights.reshape(-1)[:, None]
    combine = jnp.sum(slot_hot.reshape(local_rows, 2, experts_all * capacity), axis=1)
    summed = jnp.dot(
        combine, returned.reshape(experts_all * capacity, model_width).astype(jnp.float32)
    )
    return (stream_f + summed).astype(jnp.bfloat16)


def solution(mesh):
    finer = Mesh(mesh.devices.reshape(4, 4, 4, 2), ("z", "x", "y", "c"))
    placed = (
        P(SP, TP, None),
        P(SP, TP, None),
        P(SP, TP, None),
        P(SP, TP, None),
        P(SP, TP, None),
        P(SP, TP, None),
        P(None, TP),
        P(SP_TP, None),
        P(TP, None),
        P(TP, None),
        P(),
        P(SP_TP, None),
        P(SP_TP, None),
        P(SP_TP, None, None),
        P(SP_TP, None, None),
        P(SP_TP, None, None),
    )
    return jax.shard_map(
        shards, mesh=finer, in_specs=placed, out_specs=P(SP_TP, None), check_vma=False
    )
```

time: 605 us -> 254 us (0.42)
  matrix products: 206 us -> 26.3 us
  waiting for transfers between devices: 161 us -> 31.5 us
  Pallas kernels: 0 us -> 112 us
  local copies, waits for them, and re-layouts: 98.1 us -> 16.8 us
  other arithmetic: 40.9 us -> 2.52 us
  loops' own time: 21 us -> 0 us
  starting transfers between devices: 16.2 us -> 4.94 us
    dot_general x192 -> x0, matrix products: 180 us -> none  [the longest x96 142 us: map_update(): jnp.einsum('hqk,khv->hqv', weights.astype(jnp.bfloat16), values, preferre...]
    all_gather x1 -> x0, waiting for transfers between devices: 122 us -> none  [sent_together(): result = lax.all_gather(both, axis, axis=dim, tiled=True)]
    pallas_call x0 -> x1, Pallas kernels: none -> 112 us  [attention(): pl.pallas_call(functools.partial(attention_kernel, rows=rows), out_shape=...]
    squeeze x48 -> x0, local copies, waits for them, and re-layouts: 45.5 us -> none  [visit_piece(): lax.scan(advance, current, (jnp.arange(piece_rows // key_block, dtype=jnp...]
    reduce_sum x26 -> x0, other arithmetic: 29.4 us -> none  [the longest x24 27.3 us: map_update(): new_sum.append(factor * run_sum[which_map] + jnp.sum(weights, axis=-1))]
    another operation x2 -> x0, loops' own time: 21 us -> none  [the longest x1 21 us: visit_piece(): lax.scan(advance, current, (jnp.arange(piece_rows // key_block, dtype=jnp...]
    dynamic_slice x24 -> x0, local copies, waits for them, and re-layouts: 15.9 us -> none  [visit_piece(): lax.scan(advance, current, (jnp.arange(piece_rows // key_block, dtype=jnp...]
    split x2 -> x0, local copies, waits for them, and re-layouts: 15.7 us -> none  [sent_together(): jnp.split(result, [sum(widths[:k]) for k in range(1, len(widths))], axis=...]
  transfers between devices with their start and end apart: 7 -> 3, of which waited for: 4 -> 1; matrix products, arithmetic and copies ran while one was open for 51% -> 3% of each run, Pallas kernels for 0% -> 44%
where the time goes in v2:
time: 254 us
  Pallas kernels  112 us (44%)
  blocking collectives  46.2 us (18%)
  waiting for transfers between devices  31.5 us (12%)
  matrix products  26.3 us (10%)
  local copies, waits for them, and re-layouts  16.8 us (7%)
  between operations  13.6 us (5%)
  starting transfers between devices  4.94 us (2%)
    pallas_call x1, Pallas kernels, attention(): pl.pallas_call(functools.partial(attention_kernel, rows=rows), out_shape=...  112 us
    all_to_all x1, blocking collectives, moved(): lax.all_to_all(group, axis, split_axis=split_dim, concat_axis=concat_dim,...  46.2 us
    all_to_all x1, waiting for transfers between devices, serve_rows(): lax.all_to_all(result.reshape(sources, items, width), SP_TP, split_axis=0...  30.1 us
    dot_general x1, matrix products, serve_rows(): jnp.dot(hidden, down_weight[0], preferred_element_type=jnp.float32)  8.56 us
    reshape x1, local copies, waits for them, and re-layouts, serve_rows(): result.reshape(sources, items, width)  5.15 us
    dot_general x1, matrix products, serve_rows(): jnp.dot(flat_rows, gate_weight[0], preferred_element_type=jnp.float32)  5.15 us
  transfers between devices with their start and end apart: 3, of which 1 were waited for; matrix products, arithmetic and copies ran while one was open for 3% of the time, Pallas kernels for 44%

profile of v2, /device:TPU:1, one launch (start us, length us, event | category | flops | bytes accessed | tf_op | source)
XLA Modules:
  0.0 253.8 jit_solution(15685477736130957143)
XLA Ops:
  6.6 0.7 all-gather.3.cloned.1.call-update
  7.3 0.7 all-gather.5.cloned.1.call-update
  8.1 0.7 copy.36.lam_ref
  8.8 0.1 eq.50
  9.1 0.1 fusion.21
  9.3 0.2 fusion.24
  9.5 0.1 reduce_sum.30
  9.7 0.1 fusion.20
  9.9 0.8 pad_maximum_fusion.1.kvn_in
  10.7 1.0 pad_maximum_fusion.kvw_in
  11.7 111.9 %attention.1 = (bf16[96,2048]{1,0:T(8,128)(2,1)}, bf16[96,1024]{1,0:T(8,128)(2,1)}) custom-call(f32[2,1]{1,0:T(2,128)} %copy.36.lam_ref, bf16[768,128]{1,0:T(8,128)(2,1)} %bitcast.49, bf16[768,256]{1,0:T(8,128)(2,1)} %pad_maximum_fusion.1.kvn_in, bf16[768,256]{1,0:T(8,128)(2,1)} %bitcast.48, bf16[768,512]{1,0:T(8,128)(2,1)} %pad_maximum_fusion.kvw_in), custom_call_target="tpu_custom_call" | custom-call | flops 99999997952 | bytes 10000000 | tf_op jit(solution)/shard_map/attention/pallas_call | solution.py:398
  123.6 5.0 %fusion.26 = f32[96,2048]{1,0:T(8,128)S(1)} fusion(bf16[96,2048]{1,0:T(8,128)(2,1)} %get-tuple-element.7, bf16[2048,2048]{1,0:T(8,128)(2,1)} %all-gather.3.cloned.1.call-done), kind=kOutput, calls=%fused_computation.39 | convolution fusion | flops 805306368 | bytes 9568256 | tf_op jit(solution)/shard_map/dot_general | solution.py:467
  128.7 3.1 %multiply_reduce_fusion = (f32[96]{0:T(128)S(1)}, f32[96,2048]{1,0:T(8,128)S(1)}) fusion(bf16[96,2048]{1,0:T(8,128)(2,1)S(1)} %copy-done, f32[96,2048]{1,0:T(8,128)S(1)} %fusion.26, bf16[96,1024]{1,0:T(8,128)(2,1)S(1)} %copy-done.3, bf16[1024,2048]{1,0:T(8,128)(2,1)} %all-gather.5.cloned.1.call-done), kind=kOutput, calls=%fused_computation.18 | convolution fusion | flops 404029344 | bytes 6357376 | tf_op jit(solution)/shard_map/dot_general | solution.py:467
  131.9 1.8 convolution_convert_fusion
  133.7 4.0 %reshape.76 = bf16[128,3,2048]{2,1,0:T(4,128)(2,1)S(1)} reshape(bf16[384,2048]{1,0:T(8,128)(2,1)} %convolution_convert_fusion) | data formatting | bytes 3145728 | tf_op jit(solution)/shard_map/reshape | solution.py:492
  137.7 46.2 %all_to_all.10 = bf16[128,3,2048]{2,1,0:T(4,128)(2,1)} all-to-all(bf16[128,3,2048]{2,1,0:T(4,128)(2,1)S(1)} %reshape.76), channel_id=1, replica_groups=mesh['z'=4,'x'=4,'y'=4,'c'=2] {'z','x','y','c'}, dimensions={0} | all-to-all | bytes 3145728 | tf_op jit(solution)/shard_map/all_to_all | solution.py:426
  183.9 3.9 %reshape.77 = bf16[384,2048]{1,0:T(8,128)(2,1)S(1)} reshape(bf16[128,3,2048]{2,1,0:T(4,128)(2,1)} %all_to_all.10) | data formatting | bytes 3145728 | tf_op jit(solution)/shard_map/reshape | solution.py:496
  187.9 5.2 %fusion.4 = f32[384,1024]{1,0:T(8,128)} fusion(bf16[384,2048]{1,0:T(8,128)(2,1)S(1)} %reshape.77, bf16[1,2048,1024]{2,1,0:T(8,128)(2,1)} %param.29), kind=kOutput, calls=%fused_computation.4 | convolution fusion | flops 1610612736 | bytes 7340032 | tf_op jit(solution)/shard_map/dot_general | solution.py:497
  193.0 8.6 %fusion.6 = bf16[384,2048]{1,0:T(8,128)(2,1)} fusion(bf16[1,1024,2048]{2,1,0:T(8,128)(2,1)} %param.31, f32[384,1024]{1,0:T(8,128)} %fusion.4, bf16[384,2048]{1,0:T(8,128)(2,1)S(1)} %reshape.77, bf16[1,2048,1024]{2,1,0:T(8,128)(2,1)} %param.30), kind=kOutput, calls=%fused_computation.6 | convolution fusion | flops 3224371200 | bytes 13107200 | tf_op jit(solution)/shard_map/dot_general | solution.py:500
  201.6 5.2 %reshape.78 = bf16[128,3,2048]{2,1,0:T(4,128)(2,1)} reshape(bf16[384,2048]{1,0:T(8,128)(2,1)} %fusion.6) | data formatting | bytes 3145728 | tf_op jit(solution)/shard_map/reshape | solution.py:504
  206.7 4.9 %all-to-all-start.1 = ((bf16[128,3,2048]{2,1,0:T(4,128)(2,1)}), bf16[128,3,2048]{2,1,0:T(4,128)(2,1)S(1)}, u32[]{:S(2)}, u32[]{:S(2)}) async-start(bf16[128,3,2048]{2,1,0:T(4,128)(2,1)} %reshape.78), calls=%async_computation.1 | async-start | bytes 4194304 | tf_op jit(solution)/shard_map/all_to_all | solution.py:503
  211.8 30.1 %all-to-all-done.1 = bf16[128,3,2048]{2,1,0:T(4,128)(2,1)S(1)} async-done(((bf16[128,3,2048]{2,1,0:T(4,128)(2,1)}), bf16[128,3,2048]{2,1,0:T(4,128)(2,1)S(1)}, u32[]{:S(2)}, u32[]{:S(2)}) %all-to-all-start.1) | async-done | bytes 1572896 | tf_op jit(solution)/shard_map/all_to_all | solution.py:503
  241.9 2.5 reshape.79
  244.4 2.6 %fusion.10 = bf16[96,2048]{1,0:T(8,128)(2,1)} fusion(f32[96,2048]{1,0:T(8,128)S(1)} %get-tuple-element.10, bf16[96,384]{1,0:T(8,128)(2,1)S(1)} %select_reduce_fusion, bf16[384,2048]{1,0:T(8,128)(2,1)} %reshape.79), kind=kOutput, calls=%fused_computation.11 | convolution fusion | flops 151388160 | bytes 2826240 | tf_op jit(solution)/shard_map/dot_general | solution.py:512
  (37 shorter events, 0.6 us)
Async XLA Ops:
  6.5 1.5 copy-start.9
  6.5 2.2 copy-start.7
  6.5 3.3 %copy-start.4 = (bf16[768,1,128]{2,0,1:T(8,128)(2,1)S(1)}, bf16[768,1,128]{2,0,1:T(8,128)(2,1)}, u32[]{:S(2)}) copy-start(bf16[768,1,128]{2,0,1:T(8,128)(2,1)} %param.21) | copy-start | bytes 589828
  6.5 3.3 %copy-start.5 = (bf16[768,1,128]{2,0,1:T(8,128)(2,1)S(1)}, bf16[768,1,128]{2,0,1:T(8,128)(2,1)}, u32[]{:S(2)}) copy-start(bf16[768,1,128]{2,0,1:T(8,128)(2,1)} %param.20) | copy-start | bytes 589828
  6.5 117.0 %all-gather.3.cloned.1.call-start = ((), (), s32[]{:S(2)}) async-start(), calls=%async_computation.2 | async-start | bytes 9437184 | tf_op jit(solution)/shard_map/all_gather | solution.py:464
  7.3 3.4 %copy-start.1 = (bf16[768,1,256]{2,0,1:T(8,128)(2,1)S(1)}, bf16[768,1,256]{2,0,1:T(8,128)(2,1)}, u32[]{:S(2)}) copy-start(bf16[768,1,256]{2,0,1:T(8,128)(2,1)} %param.18) | copy-start | bytes 1179652
  7.3 3.4 %copy-start.2 = (bf16[768,1,256]{2,0,1:T(8,128)(2,1)S(1)}, bf16[768,1,256]{2,0,1:T(8,128)(2,1)}, u32[]{:S(2)}) copy-start(bf16[768,1,256]{2,0,1:T(8,128)(2,1)} %param.17) | copy-start | bytes 1179652
  7.3 121.4 %all-gather.5.cloned.1.call-start = ((), (), s32[]{:S(2)}) async-start(), calls=%async_computation.3 | async-start | bytes 4718592 | tf_op jit(solution)/shard_map/all_gather | solution.py:465
  123.6 5.1 %copy-start = (bf16[96,2048]{1,0:T(8,128)(2,1)S(1)}, bf16[96,2048]{1,0:T(8,128)(2,1)}, u32[]{:S(2)}) copy-start(bf16[96,2048]{1,0:T(8,128)(2,1)} %param.23) | copy-start | bytes 1179652
  123.6 5.1 %copy-start.3 = (bf16[96,1024]{1,0:T(8,128)(2,1)S(1)}, bf16[96,1024]{1,0:T(8,128)(2,1)}, u32[]{:S(2)}) copy-start(bf16[96,1024]{1,0:T(8,128)(2,1)} %get-tuple-element.8) | copy-start | bytes 589828
  128.7 3.2 %copy-start.6 = (f32[2048]{0:T(1024)S(1)}, f32[2048]{0:T(1024)}, u32[]{:S(2)}) copy-start(f32[2048]{0:T(1024)} %param.26) | copy-start | bytes 24580
  206.7 4.9 %copy-start.8 = (f32[96,2]{0,1:T(2,128)S(1)}, f32[96,2]{0,1:T(2,128)}, u32[]{:S(2)}) copy-start(f32[96,2]{0,1:T(2,128)} %param.28) | copy-start | bytes 2308
  206.7 35.1 %all-to-all-start.1 = ((bf16[128,3,2048]{2,1,0:T(4,128)(2,1)}), bf16[128,3,2048]{2,1,0:T(4,128)(2,1)S(1)}, u32[]{:S(2)}, u32[]{:S(2)}) async-start(bf16[128,3,2048]{2,1,0:T(4,128)(2,1)} %reshape.78), calls=%async_computation.1 | async-start | bytes 4194304 | tf_op jit(solution)/shard_map/all_to_all | solution.py:503
Sparse Core Ops, SparseCore 0:
  9.1 53.2 all-gather.2
  64.1 34.3 all-gather.4

commit v3 on v2

--- a/solution.py
+++ b/solution.py
@@ -420,20 +420,181 @@
     )(lam, qn, jnp.concatenate([kn, vn], axis=1), qw, jnp.concatenate([kw, vw], axis=1))
 
 
-def exchange_in_groups(array, axis, split_dim, concat_dim, work, item_dim, out_dim):
-
-    def moved(group):
-        return lax.all_to_all(group, axis, split_axis=split_dim, concat_axis=concat_dim, tiled=True)
-
-    items = jax.tree.leaves(array)[0].shape[item_dim]
-    ends = [items * k // 2 for k in range(2 + 1)] if items % 2 == 0 else [0, items]
-    groups = [
-        jax.tree.map(lambda a: lax.slice_in_dim(a, low, high, axis=item_dim), array)
-        for low, high in zip(ends, ends[1:])
+def device_of(e):
+    return {"z": e // 32, "x": (e // 8) % 4, "y": (e // 2) % 4, "c": e % 2}
+
+
+def swapped(perm, rows):
+    return jnp.dot(perm, rows, preferred_element_type=jnp.float32).astype(jnp.bfloat16)
+
+
+def to_tiles(perm, block):
+    width = block.shape[1] // 16
+    stacked = jnp.concatenate([block[:, g * width:(g + 1) * width] for g in range(16)], axis=0)
+    return swapped(perm, stacked).reshape(16, 16, width)
+
+
+def experts_kernel(token_ref, slot_ref, weight_ref, normed_ref, stream_ref, gate_in, up_in, down_in, out_ref,
+                   gate_s, up_s, down_s, perm_s, rows_s, stream_s, send_s, got_s, flat_s, hidden_s, back_s,
+                   weight_sems, send_sems, recv_sems, send2_sems, recv2_sems):
+    count = 128
+    cap = send_s.shape[0] // count
+    total = send_s.shape[0]
+    tokens = normed_ref.shape[0]
+    me = ((lax.axis_index("z") * 4 + lax.axis_index("x")) * 4 + lax.axis_index("y")) * 2 + lax.axis_index("c")
+    loads = [
+        pltpu.make_async_copy(src.at[0], dst, weight_sems.at[n])
+        for n, (src, dst) in enumerate(((gate_in, gate_s), (up_in, up_s), (down_in, down_s)))
     ]
-    arrived = [moved(group) for group in groups]
-    made = [work(group) for group in arrived]
-    return jax.tree.map(lambda *parts: jnp.concatenate(parts, axis=out_dim), *made)
+    for c in loads:
+        c.start()
+    barrier = pltpu.get_barrier_semaphore()
+
+    def greet(k, _):
+        pl.semaphore_signal(barrier, inc=1, device_id=device_of((me + k) % count), device_id_type=pl.DeviceIdType.MESH)
+        return 0
+    lax.fori_loop(1, count, greet, 0)
+
+    r = lax.broadcasted_iota(jnp.int32, (256, 256), 0)
+    c = lax.broadcasted_iota(jnp.int32, (256, 256), 1)
+    perm_s[...] = jnp.where((r % 16) * 16 + r // 16 == c, 1.0, 0.0).astype(jnp.bfloat16)
+    perm = perm_s[...]
+    for b in range(tokens // 16):
+        s = slice(b * 16, (b + 1) * 16)
+        rows_s[s] = to_tiles(perm, normed_ref[s])
+
+    def fill(n, _):
+        for u in range(8):
+            send_s[n * 8 + u] = rows_s[token_ref[n * 8 + u]]
+        return 0
+    lax.fori_loop(0, total // 8, fill, 0)
+    pl.semaphore_wait(barrier, count - 1)
+
+    def copy(src, dst, sends, recvs, k):
+        e = (me + k) % count
+        return pltpu.make_async_remote_copy(
+            src_ref=src.at[pl.ds(e * cap, cap)],
+            dst_ref=dst.at[pl.ds(me * cap, cap)],
+            send_sem=sends.at[k],
+            recv_sem=recvs.at[k],
+            device_id=device_of(e),
+            device_id_type=pl.DeviceIdType.MESH,
+        )
+
+    def exchange(src, dst, sends, recvs):
+        def go(k, _):
+            copy(src, dst, sends, recvs, k).start()
+            return 0
+        lax.fori_loop(1, count, go, 0)
+        dst[pl.ds(me * cap, cap)] = src[pl.ds(me * cap, cap)]
+
+    def arrive(src, dst, sends, recvs):
+        def done(k, _):
+            copy(src, dst, sends, recvs, k).wait_recv()
+            return 0
+        lax.fori_loop(1, count, done, 0)
+
+    def leave(src, dst, sends, recvs):
+        def done(k, _):
+            copy(src, dst, sends, recvs, k).wait_send()
+            return 0
+        lax.fori_loop(1, count, done, 0)
+
+    there = (send_s, got_s, send_sems, recv_sems)
+    exchange(*there)
+    for b in range(tokens // 16):
+        s = slice(b * 16, (b + 1) * 16)
+        stream_s[s] = to_tiles(perm, stream_ref[s])
+    for c in loads:
+        c.wait()
+    arrive(*there)
+
+    def flatten(n, _):
+        for u in range(4):
+            at = pl.multiple_of((n * 4 + u) * 16, 16)
+            turned = swapped(perm, got_s[pl.ds(at, 16)].reshape(256, 128))
+            for g in range(16):
+                flat_s[pl.ds(at, 16), g * 128:(g + 1) * 128] = turned[g * 16:(g + 1) * 16]
+        return 0
+    lax.fori_loop(0, total // 64, flatten, 0)
+
+    def first(n, _):
+        at = pl.ds(pl.multiple_of(n * 256, 256), 256)
+        gate = jnp.dot(flat_s[...], gate_s[:, at], preferred_element_type=jnp.float32)
+        up = jnp.dot(flat_s[...], up_s[:, at], preferred_element_type=jnp.float32)
+        hidden_s[:, at] = (gate * jax.nn.sigmoid(gate) * up).astype(jnp.bfloat16)
+        return 0
+    lax.fori_loop(0, hidden_s.shape[1] // 256, first, 0)
+
+    def second(n, _):
+        at = pl.ds(pl.multiple_of(n * 256, 256), 256)
+        flat_s[:, at] = jnp.dot(hidden_s[...], down_s[:, at], preferred_element_type=jnp.float32).astype(jnp.bfloat16)
+        return 0
+    lax.fori_loop(0, flat_s.shape[1] // 256, second, 0)
+    leave(*there)
+
+    def unflatten(n, _):
+        for u in range(4):
+            at = pl.ds(pl.multiple_of((n * 4 + u) * 16, 16), 16)
+            send_s[at] = to_tiles(perm, flat_s[at, :])
+        return 0
+    lax.fori_loop(0, total // 64, unflatten, 0)
+
+    back = (send_s, back_s, send2_sems, recv2_sems)
+    exchange(*back)
+    arrive(*back)
+
+    def combine(n, _):
+        for u in range(4):
+            t = n * 4 + u
+            summed = weight_ref[2 * t] * back_s[slot_ref[2 * t]].astype(jnp.float32)
+            summed = summed + weight_ref[2 * t + 1] * back_s[slot_ref[2 * t + 1]].astype(jnp.float32)
+            rows_s[t] = (stream_s[t].astype(jnp.float32) + summed).astype(jnp.bfloat16)
+        return 0
+    lax.fori_loop(0, tokens // 4, combine, 0)
+    for b in range(tokens // 16):
+        s = slice(b * 16, (b + 1) * 16)
+        turned = swapped(perm, rows_s[s].reshape(256, 128))
+        for g in range(16):
+            out_ref[s, g * 128:(g + 1) * 128] = turned[g * 16:(g + 1) * 16]
+    leave(*back)
+
+
+def experts(token_of_slot, slot_of_token, weight, normed, stream, gate, up, down):
+    tokens, width = normed.shape
+    slots = token_of_slot.shape[0]
+    inner = gate.shape[2]
+    smem = pl.BlockSpec(memory_space=pltpu.SMEM)
+    vmem = pl.BlockSpec(memory_space=pltpu.VMEM)
+    any_ = pl.BlockSpec(memory_space=pl.ANY)
+    bf16 = jnp.bfloat16
+    return pl.pallas_call(
+        experts_kernel,
+        out_shape=jax.ShapeDtypeStruct((tokens, width), bf16),
+        in_specs=[smem] * 3 + [vmem] * 2 + [any_] * 3,
+        out_specs=vmem,
+        scratch_shapes=[
+            pltpu.VMEM((width, inner), bf16),
+            pltpu.VMEM((width, inner), bf16),
+            pltpu.VMEM((inner, width), bf16),
+            pltpu.VMEM((256, 256), bf16),
+            pltpu.VMEM((tokens, 16, width // 16), bf16),
+            pltpu.VMEM((tokens, 16, width // 16), bf16),
+            pltpu.VMEM((slots, 16, width // 16), bf16),
+            pltpu.VMEM((slots, 16, width // 16), bf16),
+            pltpu.VMEM((slots, width), bf16),
+            pltpu.VMEM((slots, inner), bf16),
+            pltpu.VMEM((slots, 16, width // 16), bf16),
+            pltpu.SemaphoreType.DMA((3,)),
+            pltpu.SemaphoreType.DMA((128,)),
+            pltpu.SemaphoreType.DMA((128,)),
+            pltpu.SemaphoreType.DMA((128,)),
+            pltpu.SemaphoreType.DMA((128,)),
+        ],
+        name="experts",
+        cost_estimate=pl.CostEstimate(flops=50 * 10**9, bytes_accessed=2 * 10**7, transcendentals=0),
+        compiler_params=pltpu.CompilerParams(collective_id=1, has_side_effects=True, vmem_limit_bytes=60 * 2**20),
+    )(token_of_slot, slot_of_token, weight, normed, stream, gate, up, down)
 
 
 def shards(
@@ -476,7 +637,6 @@
     ).astype(jnp.bfloat16)
     experts_all = lax.axis_size(SP) * tp_size
     capacity = max(2, 4 * local_rows // experts_all)
-    model_width = normed.shape[1]
     flat_expert = expert_ids.reshape(-1)
     expert_hot = (flat_expert[:, None] == jnp.arange(experts_all, dtype=jnp.int32)[None, :]).astype(
         jnp.int32
@@ -485,34 +645,11 @@
     flat_slot = flat_expert * capacity + slot_rank
     slot_ids = jnp.arange(experts_all * capacity, dtype=jnp.int32)
     placed = slot_ids[:, None] == flat_slot[None, :]
-    dispatch = jnp.any(placed.reshape(experts_all * capacity, local_rows, 2), axis=2).astype(
-        jnp.bfloat16
+    token = jnp.arange(2 * local_rows, dtype=jnp.int32) // 2
+    token_of_slot = jnp.max(jnp.where(placed, token[None, :], 0), axis=1)
+    return experts(
+        token_of_slot, flat_slot, expert_weights.reshape(-1), normed, stream, gate_weight, up_weight, down_weight
     )
-    outgoing = jnp.dot(dispatch, normed, preferred_element_type=jnp.float32).astype(jnp.bfloat16)
-    outgoing = outgoing.reshape(experts_all, capacity, model_width)
-
-    def serve_rows(arrived):
-        sources, items, width = arrived.shape
-        flat_rows = arrived.reshape(sources * items, width)
-        gate_part = jnp.dot(flat_rows, gate_weight[0], preferred_element_type=jnp.float32)
-        up_part = jnp.dot(flat_rows, up_weight[0], preferred_element_type=jnp.float32)
-        hidden = (jax.nn.silu(gate_part) * up_part).astype(jnp.bfloat16)
-        result = jnp.dot(hidden, down_weight[0], preferred_element_type=jnp.float32).astype(
-            jnp.bfloat16
-        )
-        return lax.all_to_all(
-            result.reshape(sources, items, width), SP_TP, split_axis=0, concat_axis=0, tiled=True
-        )
-
-    returned = exchange_in_groups(outgoing, SP_TP, 0, 0, serve_rows, 1, 1)
-    slot_hot = (flat_slot[:, None] == slot_ids[None, :]).astype(
-        jnp.float32
-    ) * expert_weights.reshape(-1)[:, None]
-    combine = jnp.sum(slot_hot.reshape(local_rows, 2, experts_all * capacity), axis=1)
-    summed = jnp.dot(
-        combine, returned.reshape(experts_all * capacity, model_width).astype(jnp.float32)
-    )
-    return (stream_f + summed).astype(jnp.bfloat16)
 
 
 def solution(mesh):

time: 254 us -> 234 us (0.921)
  Pallas kernels: 112 us -> 200 us
  blocking collectives: 46.2 us -> 0 us
  waiting for transfers between devices: 31.5 us -> 1.45 us
  matrix products: 26.3 us -> 8.17 us
  local copies, waits for them, and re-layouts: 16.8 us -> 5.57 us
  starting transfers between devices: 4.94 us -> 0.04 us
    pallas_call x0 -> x1, Pallas kernels: none -> 87.5 us  [experts(): pl.pallas_call(experts_kernel, out_shape=jax.ShapeDtypeStruct((tokens, wi...]
    all_to_all x1 -> x0, blocking collectives: 46.2 us -> none  [moved(): lax.all_to_all(group, axis, split_axis=split_dim, concat_axis=concat_dim,...]
    all_to_all x1 -> x0, waiting for transfers between devices: 30.1 us -> none  [serve_rows(): lax.all_to_all(result.reshape(sources, items, width), SP_TP, split_axis=0...]
    dot_general x4 -> x0, matrix products: 18.1 us -> none  [the longest x1 8.56 us: serve_rows(): jnp.dot(hidden, down_weight[0], preferred_element_type=jnp.float32)]
    reshape x4 -> x2, local copies, waits for them, and re-layouts: 15.6 us -> 0.87 us  [the longest x1 0.73 us: shards(): expert_weights.reshape(-1)]
    all_to_all x1 -> x0, starting transfers between devices: 4.87 us -> none  [serve_rows(): lax.all_to_all(result.reshape(sources, items, width), SP_TP, split_axis=0...]
    unnamed x23 -> x19, local copies, waits for them, and re-layouts: 0.83 us -> 4.68 us
  transfers between devices with their start and end apart: 3 -> 2, of which waited for: 1 -> 0; matrix products, arithmetic and copies ran while one was open for 3% -> 6% of each run, Pallas kernels for 44% -> 48%
where the time goes in v3:
time: 234 us; the launch traced here: 233 us
  Pallas kernels  200 us (85%)
  between operations  13.6 us (6%)
  matrix products  8.17 us (3%)
  local copies, waits for them, and re-layouts  5.57 us (2%)
  other arithmetic  5 us (2%)
    pallas_call x1, Pallas kernels, attention(): pl.pallas_call(functools.partial(attention_kernel, rows=rows), out_shape=...  112 us
    pallas_call x1, Pallas kernels, experts(): pl.pallas_call(experts_kernel, out_shape=jax.ShapeDtypeStruct((tokens, wi...  87.5 us
    dot_general x1, matrix products, shards(): jnp.dot(mine_wide, whole_wide, preferred_element_type=jnp.float32)  5.02 us
    unnamed x19, local copies, waits for them, and re-layouts  4.68 us
  transfers between devices with their start and end apart: 2, of which 0 were waited for; matrix products, arithmetic and copies ran while one was open for 6% of the time, Pallas kernels for 48%

profile of v3, /device:TPU:1, one launch (start us, length us, event | category | flops | bytes accessed | tf_op | source)
XLA Modules:
  0.0 233.5 jit_solution(7427762451344363023)
XLA Ops:
  6.5 0.7 all-gather.3.cloned.1.call-update
  7.3 0.0 all-gather.5.cloned.1.call-start
  7.3 0.7 all-gather.5.cloned.1.call-update
  8.0 0.8 copy.23
  8.8 0.1 reshape.48
  8.9 0.1 iota_compare_fusion.1
  9.0 0.1 fusion.5
  9.3 0.2 fusion.8
  9.5 1.3 copy.27.lam_ref
  10.8 0.8 copy.26
  11.6 0.7 reshape.51.weight_ref
  12.3 0.7 select_reduce_fusion.token_ref
  13.0 2.1 pad_maximum_fusion.kvw_in
  15.1 0.8 pad_maximum_fusion.1.kvn_in
  15.9 112.2 %attention.1 = (bf16[96,2048]{1,0:T(8,128)(2,1)}, bf16[96,1024]{1,0:T(8,128)(2,1)}) custom-call(f32[2,1]{1,0:T(2,128)} %copy.27.lam_ref, bf16[768,128]{1,0:T(8,128)(2,1)} %bitcast.29, bf16[768,256]{1,0:T(8,128)(2,1)} %pad_maximum_fusion.1.kvn_in, bf16[768,256]{1,0:T(8,128)(2,1)} %bitcast.28, bf16[768,512]{1,0:T(8,128)(2,1)} %pad_maximum_fusion.kvw_in), custom_call_target="tpu_custom_call" | custom-call | flops 99999997952 | bytes 10000000 | tf_op jit(solution)/shard_map/attention/pallas_call | solution.py:398
  128.2 0.0 all-gather.3.cloned.1.call-done
  128.2 0.0 copy-start.1
  128.2 5.0 %fusion.9 = f32[96,2048]{1,0:T(8,128)S(1)} fusion(bf16[96,2048]{1,0:T(8,128)(2,1)} %get-tuple-element.7, bf16[2048,2048]{1,0:T(8,128)(2,1)} %all-gather.3.cloned.1.call-done), kind=kOutput, calls=%fused_computation.28 | convolution fusion | flops 805306368 | bytes 9568256 | tf_op jit(solution)/shard_map/dot_general | solution.py:628
  133.3 0.0 copy-start.5
  133.3 0.0 all-gather.5.cloned.1.call-done
  133.3 3.1 %fusion.2 = (f32[96]{0:T(128)S(1)}, bf16[96,2048]{1,0:T(8,128)(2,1)S(1)}) fusion(bf16[96,2048]{1,0:T(8,128)(2,1)S(1)} %copy-done.1, f32[96,2048]{1,0:T(8,128)S(1)} %fusion.9, bf16[96,1024]{1,0:T(8,128)(2,1)S(1)} %copy-done.2, bf16[1024,2048]{1,0:T(8,128)(2,1)} %all-gather.5.cloned.1.call-done), kind=kOutput, calls=%fused_computation.5 | convolution fusion | flops 404029344 | bytes 5964160 | tf_op jit(solution)/shard_map/dot_general | solution.py:628
  136.5 0.9 fusion.4.normed_ref
  137.4 87.5 %experts.1 = bf16[96,2048]{1,0:T(8,128)(2,1)} custom-call(s32[384]{0:T(512)} %select_reduce_fusion.token_ref, s32[192]{0:T(256)} %copy-done.6, f32[192]{0:T(256)} %reshape.51.weight_ref, bf16[96,2048]{1,0:T(8,128)(2,1)} %fusion.4.normed_ref, bf16[96,2048]{1,0:T(8,128)(2,1)} %copy-done, bf16[1,2048,1024]{2,1,0:T(8,128)(2,1)} %gate_in.1, ...), custom_call_target="tpu_custom_call" | custom-call | flops 49999998976 | bytes 20000000 | tf_op jit(solution)/shard_map/experts/pallas_call | solution.py:571
  224.9 1.8 copy.31
  (22 shorter events, 0.1 us)
Async XLA Ops:
  6.5 8.6 %copy-start.4 = (bf16[768,1,128]{2,0,1:T(8,128)(2,1)S(1)}, bf16[768,1,128]{2,0,1:T(8,128)(2,1)}, u32[]{:S(2)}) copy-start(bf16[768,1,128]{2,0,1:T(8,128)(2,1)} %param.20) | copy-start | bytes 589828
  6.5 8.6 %copy-start.3 = (bf16[768,1,128]{2,0,1:T(8,128)(2,1)S(1)}, bf16[768,1,128]{2,0,1:T(8,128)(2,1)}, u32[]{:S(2)}) copy-start(bf16[768,1,128]{2,0,1:T(8,128)(2,1)} %param.21) | copy-start | bytes 589828
  6.5 121.7 %all-gather.3.cloned.1.call-start = ((), (), s32[]{:S(2)}) async-start(), calls=%async_computation | async-start | bytes 9437184 | tf_op jit(solution)/shard_map/all_gather | solution.py:625
  7.3 126.0 %all-gather.5.cloned.1.call-start = ((), (), s32[]{:S(2)}) async-start(), calls=%async_computation.1 | async-start | bytes 4718592 | tf_op jit(solution)/shard_map/all_gather | solution.py:626
  9.5 118.7 %copy-start.6 = (s32[192]{0:T(256)}, s32[192]{0:T(256)S(1)}, u32[]{:S(2)}) copy-start(s32[192]{0:T(256)S(1)} %get-tuple-element.12.slot_ref) | copy-start | bytes 2308
  128.2 5.1 %copy-start.1 = (bf16[96,2048]{1,0:T(8,128)(2,1)S(1)}, bf16[96,2048]{1,0:T(8,128)(2,1)}, u32[]{:S(2)}) copy-start(bf16[96,2048]{1,0:T(8,128)(2,1)} %param.23) | copy-start | bytes 1179652
  128.2 5.1 %copy-start.2 = (bf16[96,1024]{1,0:T(8,128)(2,1)S(1)}, bf16[96,1024]{1,0:T(8,128)(2,1)}, u32[]{:S(2)}) copy-start(bf16[96,1024]{1,0:T(8,128)(2,1)} %get-tuple-element.8) | copy-start | bytes 589828
  133.3 3.2 %copy-start.5 = (f32[2048]{0:T(1024)S(1)}, f32[2048]{0:T(1024)}, u32[]{:S(2)}) copy-start(f32[2048]{0:T(1024)} %param.26) | copy-start | bytes 24580
  136.5 0.9 copy-start
Sparse Core Ops, SparseCore 0:
  9.0 53.2 all-gather.2
  64.1 33.8 all-gather.4

commit v4 on v3

v4 whole, which is shorter than its diff:
```python
import functools
import jax
import jax.numpy as jnp
from jax import lax
from jax.experimental import pallas as pl
from jax.experimental.pallas import tpu as pltpu
from jax.sharding import Mesh
from jax.sharding import PartitionSpec as P

TP = ("y", "c")
SP = ("z", "x")
SP_TP = ("z", "x", "y", "c")

NEG = -1e30
LOG2E = 1.4426950408889634
TQ = 256
CH = 256
SHIFTS = (0, 1, 3, 2)
SLOT = {t: i for i, t in enumerate(SHIFTS)}


class Copies:
    def __init__(self, send_sems, recv_sems):
        self.send_sems, self.recv_sems, self.count, self.all = send_sems, recv_sems, 0, []

    def one(self, src, dst, send, recv, device):
        return pltpu.make_async_remote_copy(
            src_ref=src,
            dst_ref=dst,
            send_sem=self.send_sems.at[send],
            recv_sem=self.recv_sems.at[recv],
            device_id=device,
            device_id_type=pl.DeviceIdType.MESH,
        )

    def make(self, src, dst, **device):
        copy = self.one(src, dst, self.count, self.count, device)
        self.count += 1
        self.all.append(copy)
        return copy


class Heads:
    def __init__(self, d, dv, rows, groups, ins, refs, kv_pair, shared, copies):
        self.d, self.dv, self.rows, self.half, self.groups = d, dv, rows, rows // 2, groups
        self.q_in, self.k_in, self.v_in = ins
        self.q_s, self.kv_s, self.qt_s, self.vt_s, self.acc, self.m_s, self.l_s, self.st, self.st_in, self.part, self.part_in, self.relay, self.heads, self.out = refs
        self.kv = kv_pair
        self.tab, self.pos, self.s_a, self.s_b, self.t_a, self.t_b, self.p_scr = shared
        self.scale = d ** (-0.5) * LOG2E
        self.copies = copies
        z, x = lax.axis_index("z"), lax.axis_index("x")
        up = {"z": (z + 1) % 4}, {"z": (z + 3) % 4}
        right = {"x": (x + 1) % 4}, {"x": (x + 3) % 4}
        half = self.half
        one, three, two = SLOT[1], SLOT[3], SLOT[2]
        h0, h1 = pl.ds(0, half), pl.ds(half, half)
        lanes = (self.k_in, pl.ds(0, 2 * d)), (self.v_in, pl.ds(2 * d, dv))
        self.q_near = [copies.make(self.q_in, self.q_s.at[one], **up[0]), copies.make(self.q_in, self.q_s.at[three], **up[1])]
        self.q_far = [
            copies.make(self.q_s.at[one, h0], self.q_s.at[two, h0], **up[0]),
            copies.make(self.q_s.at[three, h1], self.q_s.at[two, h1], **up[1]),
        ]
        self.swap = [copies.make(src.at[h1], self.kv_at(1, 0, slice(None), at), z=3 - z) for src, at in lanes]
        self.own = [(src.at[h0], self.kv_at(0, 0, slice(None), at)) for src, at in lanes] + [(self.q_in, self.q_s.at[0])]
        quarter = half // 2
        g0, g1 = pl.ds(0, quarter), pl.ds(quarter, quarter)
        self.kv_near = [
            [[copies.make(src.at[h0], self.kv_at(0, slot, slice(None), at), **to) for src, at in lanes] for slot, to in ((one, right[0]), (three, right[1]))],
            [[copies.make(self.kv_at(1, 0), self.kv_at(1, slot), **to)] for slot, to in ((one, right[0]), (three, right[1]))],
        ]
        self.kv_far = [[
            copies.make(self.kv_at(b, one, g0), self.kv_at(b, two, g0), **right[0]),
            copies.make(self.kv_at(b, three, g1), self.kv_at(b, two, g1), **right[1]),
        ] for b in range(2)]
        self.st_out, self.part_near, self.part_first, self.part_far = [], [], [], []
        for p0, p1 in groups:
            cols = pl.ds(p0 * 4 * TQ, (p1 - p0) * 4 * TQ)
            self.st_out.append([copies.make(self.st.at[:, cols], self.st_in.at[t - 1, :, cols], z=(z + t) % 4) for t in (1, 2, 3)])
            size = (p1 - p0) * TQ
            all_, f0, f1 = pl.ds(p0 * TQ, size), pl.ds(p0 * TQ, size // 2), pl.ds(p0 * TQ + size // 2, size // 2)
            held = pl.ds(p0 * TQ // 2, size // 2)
            self.part_near.append([
                copies.make(self.part.at[one, all_], self.part_in.at[0, all_], **up[1]),
                copies.make(self.part.at[three, all_], self.part_in.at[1, all_], **up[0]),
            ])
            self.part_first.append([
                copies.make(self.part.at[two, f0], self.relay.at[0, held], **up[0]),
                copies.make(self.part.at[two, f1], self.relay.at[1, held], **up[1]),
            ])
            self.part_far.append([
                copies.make(self.relay.at[0, held], self.part_in.at[2, f0], **up[0]),
                copies.make(self.relay.at[1, held], self.part_in.at[2, f1], **up[1]),
            ])
        self.rank = lax.axis_index("y") * 2 + lax.axis_index("c")
        self.base = copies.count
        copies.count += 8

    def kv_at(self, b, *index):
        ref = self.kv[b] if self.kv else self.kv_s
        index = index if self.kv else (b,) + index
        return ref.at[index] if index else ref

    def to_token(self, r):
        mine = self.rows // 8
        at = pl.multiple_of(self.rank * self.dv, self.dv)
        return self.copies.one(
            self.heads.at[pl.ds(r * mine, mine)], self.out.at[:, pl.ds(at, self.dv)],
            self.base + r, self.base + self.rank, {"y": r // 2, "c": r % 2},
        )

    def from_rank(self, r):
        mine = self.rows // 8
        return self.copies.one(
            self.heads.at[pl.ds(r * mine, mine)], self.out.at[:, r * self.dv:(r + 1) * self.dv],
            self.base + r, self.base + r, {"y": r // 2, "c": r % 2},
        )

    def send_swap(self):
        for c in self.swap:
            c.start()

    def send_near(self):
        for c in self.kv_near[0][0] + self.kv_near[0][1] + self.q_near:
            c.start()

    def pass_swap(self):
        for c in self.swap:
            c.wait_recv()
        for near in self.kv_near[1]:
            near[0].start()

    def relay_queries(self):
        for near, far in zip(self.q_near, self.q_far):
            near.wait_recv()
            far.start()

    def relay_keys(self, b):
        for near, far in zip(self.kv_near[b], self.kv_far[b]):
            for c in near:
                c.wait_recv()
            far.start()

    def clear(self):
        self.m_s[...] = jnp.full_like(self.m_s, NEG)
        self.l_s[...] = jnp.zeros_like(self.l_s)

        def tile(n, _):
            self.acc[:, :, pl.ds(pl.multiple_of(n * TQ, TQ), TQ)] = jnp.zeros((2, self.dv, TQ), jnp.float32)
            return 0
        lax.fori_loop(0, 4 * self.rows // TQ, tile, 0)

    def turn_queries(self):
        for c in self.q_far:
            c.wait_recv()

        def turn(i, _):
            for p in range(self.rows // TQ):
                at = pl.multiple_of((p * 4 + i) * TQ, TQ)
                self.qt_s[:, pl.ds(at, TQ)] = self.q_s[i, p * TQ:(p + 1) * TQ].T
            return 0
        lax.fori_loop(0, 4, turn, 0)

    def wait_values(self, b):
        for c in self.kv_far[b]:
            c.wait_recv()

    def turn_values(self, b):
        d, dv, half = self.d, self.dv, self.half

        def turn(i, _):
            at = pl.multiple_of((b * 4 + i) * half, half)
            self.vt_s[:, pl.ds(at, half)] = self.kv_at(b)[i, :, 2 * d:2 * d + dv].T
            return 0
        lax.fori_loop(0, 4, turn, 0)

    def read(self, i, s_buf, t_buf, b=None):
        d, half = self.d, self.half
        q0 = pl.multiple_of(self.tab[0, i] * TQ, TQ)
        kj = self.tab[1, i]
        part, first = kj // 2, (kj % 2) * 2
        for w in range(2):
            qt = self.qt_s[w * d:(w + 1) * d, pl.ds(q0, TQ)]
            top = None
            for c in range(2):
                lanes = slice(w * d, (w + 1) * d)
                k = self.kv_s[part, first + c, :, lanes] if b is None else self.kv[b][first + c, :, lanes]
                s = jnp.dot(k, qt, preferred_element_type=jnp.float32)
                s_buf[w, c * half:(c + 1) * half] = s
                m8 = jnp.max(s.reshape(half // 8, 8, TQ), axis=0)
                top = m8 if top is None else jnp.maximum(top, m8)
            t_buf[w] = top

    def mask(self, i, s_buf, t_buf):
        rows, half = self.rows, self.half
        qi, kj = self.tab[0, i], self.tab[1, i]
        qp = self.pos[qi % 4] + (qi // 4) * TQ
        CM = 128
        t_buf[...] = jnp.full_like(t_buf, NEG)

        def chunk(c, _):
            r = pl.multiple_of(c * CM, CM)
            late = c // (half // CM)
            k0 = self.pos[4 + 2 * kj + late] + (c - late * (half // CM)) * CM
            keep = lax.broadcasted_iota(jnp.int32, (CM, TQ), 0) - lax.broadcasted_iota(jnp.int32, (CM, TQ), 1) <= qp - k0
            for w in range(2):
                s = jnp.where(keep, s_buf[w, pl.ds(r, CM)], NEG)
                s_buf[w, pl.ds(r, CM)] = s
                t_buf[w] = jnp.maximum(t_buf[w], jnp.max(s.reshape(CM // 8, 8, TQ), axis=0))
            return 0
        lax.fori_loop(0, rows // CM, chunk, 0)

    def weigh(self, i, s_buf, t_buf):
        rows = self.rows
        cols = pl.ds(pl.multiple_of(self.tab[0, i] * TQ, TQ), TQ)
        k0 = pl.multiple_of(self.tab[1, i] * rows, rows)
        for w in range(2):
            old = self.m_s[w:w + 1, cols]
            new = jnp.maximum(old, jnp.max(t_buf[w], axis=0, keepdims=True) * self.scale)
            f = jnp.exp2(old - new)
            self.m_s[w:w + 1, cols] = new
            tot = None
            for c in range(rows // CH):
                p = jnp.exp2(s_buf[w, c * CH:(c + 1) * CH] * self.scale - new)
                t8 = jnp.sum(p.reshape(CH // 8, 8, TQ), axis=0)
                tot = t8 if tot is None else tot + t8
                self.p_scr[w, c * CH:(c + 1) * CH] = p.astype(jnp.bfloat16)
            o = jnp.dot(self.vt_s[:, pl.ds(k0, rows)], self.p_scr[w], preferred_element_type=jnp.float32)
            self.l_s[w, :, cols] = self.l_s[w, :, cols] * f + tot
            self.acc[w, :, cols] = self.acc[w, :, cols] * f + o

    def run(self, low, high, hooks, b=None):
        def advance(i, cur, nxt):
            @pl.when(self.tab[2, i] == 1)
            def _():
                self.mask(i, *cur)
            self.read(jnp.minimum(i + 1, high - 1), *nxt, b)
            self.weigh(i, *cur)

        one, two = (self.s_a, self.t_a), (self.s_b, self.t_b)
        self.read(low, *one, b)
        turns = jnp.maximum((high - low + 1) // 2, len(hooks) + 1)

        def pair(n, _):
            for k, hook in enumerate(hooks):
                pl.when(n == turns * (k + 1) // (len(hooks) + 1))(hook)
            i = low + 2 * n

            @pl.when(i < high)
            def _():
                advance(i, one, two)

            @pl.when(i + 1 < high)
            def _():
                advance(i + 1, two, one)
            return 0
        lax.fori_loop(0, turns, pair, 0)

    def mix(self, g, slot, lam):
        dv = self.dv
        for p in range(*self.groups[g]):
            c0 = (p * 4 + slot) * TQ
            stats = [self.st[:, c0:c0 + TQ]]
            for t in (1, 2, 3):
                at = (p * 4 + SLOT[(SHIFTS[slot] - t) % 4]) * TQ
                stats.append(self.st_in[t - 1, :, at:at + TQ])
            weights = []
            for w in range(2):
                peaks = [s[w:w + 1] for s in stats]
                top = functools.reduce(jnp.maximum, peaks)
                total = sum(s[2 + w:3 + w] * jnp.exp2(m - top) for m, s in zip(peaks, stats))
                weights.append(jnp.exp2(peaks[0] - top) / total)
            mixed = self.acc[0, :, c0:c0 + TQ] * weights[0] - self.acc[1, :, c0:c0 + TQ] * (weights[1] * lam)
            self.part[slot, p * TQ:(p + 1) * TQ] = mixed.T.astype(jnp.bfloat16)

    def send_stats(self, g):
        p0, p1 = self.groups[g]
        cols = slice(p0 * 4 * TQ, p1 * 4 * TQ)
        self.st[0:2, cols] = self.m_s[:, cols]
        for w in range(2):
            self.st[2 + w:3 + w, cols] = jnp.sum(self.l_s[w, :, cols], axis=0, keepdims=True)
        for c in self.st_out[g]:
            c.start()

    def mix_and_send(self, g, lam):
        for c in self.st_out[g]:
            c.wait_recv()
        self.mix(g, SLOT[2], lam)
        for c in self.part_first[g]:
            c.start()
        self.mix(g, SLOT[1], lam)
        self.part_near[g][0].start()
        self.mix(g, SLOT[3], lam)
        self.part_near[g][1].start()

    def pass_parts(self, g):
        for first, far in zip(self.part_first[g], self.part_far[g]):
            first.wait_recv()
            far.start()

    def finish(self, g, lam):
        self.mix(g, 0, lam)
        for c in self.part_near[g] + self.part_far[g]:
            c.wait_recv()
        B = 128
        p0, p1 = self.groups[g]
        for at in range(p0 * TQ, p1 * TQ, B):
            r = slice(at, at + B)
            total = self.part[0, r].astype(jnp.float32)
            for n in range(3):
                total = total + self.part_in[n, r].astype(jnp.float32)
            total = total * lax.rsqrt(jnp.mean(total * total, axis=-1, keepdims=True) + 1e-06)
            self.heads[r] = total.astype(jnp.bfloat16)
        mine = self.rows // 8
        for r in range(8):
            if p0 * TQ < (r + 1) * mine <= p1 * TQ:
                pl.when(r != self.rank)(self.to_token(r).start)


class Weights:
    def __init__(self, ins, sizes, held, copies):
        self.held = held
        y, c = lax.axis_index("y"), lax.axis_index("c")
        up, down, pair = {"y": (y + 1) % 4}, {"y": (y + 3) % 4}, {"c": 1 - c}
        self.own, self.first, self.near, self.far, self.pass_near, self.pass_far = [], [], [], [], [], []
        base = 0
        for src, size in zip(ins, sizes):
            half = size // 2

            def rows(t, at=0, n=size, base=base, size=size):
                return held.at[pl.ds(pl.multiple_of(base + (((y + t) % 4) * 2 + c) * size + at, half), n)]
            self.own.append((src, rows(0)))
            self.first.append(copies.make(src, rows(0), **pair))
            self.near.append([copies.make(src, rows(0), **up), copies.make(src, rows(0), **down)])
            self.far.append([
                copies.make(rows(3, 0, half), rows(3, 0, half), **up),
                copies.make(rows(1, half, half), rows(1, half, half), **down),
            ])
            self.pass_near.append([copies.make(rows(3), rows(3), **pair), copies.make(rows(1), rows(1), **pair)])
            self.pass_far.append([copies.make(rows(2, 0, half), rows(2, 0, half), **pair), copies.make(rows(2, half, half), rows(2, half, half), **pair)])
            base += 8 * size

    def send(self):
        for near, first in zip(self.near, self.first):
            for c in near:
                c.start()
            first.start()

    def relay(self):
        for near, far, onward in zip(self.near, self.far, self.pass_near):
            for n, f, o in zip(near, far, onward):
                n.wait_recv()
                f.start()
                o.start()

    def last(self):
        for far, onward in zip(self.far, self.pass_far):
            for f, o in zip(far, onward):
                f.wait_recv()
                o.start()

    def wait(self):
        for c in self.first:
            c.wait_recv()
        for group in self.pass_near + self.pass_far:
            for c in group:
                c.wait_recv()


def attention_kernel(lam_ref, residual_ref, gain_ref, ow_in, on_in, qn_in, kn_in, vn_in, qw_in, kw_in, vw_in, stream_ref, normed_ref, *scratch, rows):
    narrow_refs, wide_refs = scratch[:14], scratch[14:28]
    shared, (send_sems, recv_sems, local_sems, weights_s, sum_s) = scratch[28:35], scratch[35:40]
    z, x = lax.axis_index("z"), lax.axis_index("x")
    half = rows // 2
    per = rows // TQ
    copies = Copies(send_sems, recv_sems)
    narrow = Heads(64, 128, rows, ((0, per - 1), (per - 1, per)), (qn_in, kn_in, vn_in), narrow_refs, None, shared, copies)
    wide = Heads(128, 256, rows, ((0, per),), (qw_in, kw_in, vw_in), wide_refs, scratch[40:42], shared, copies)
    weights = Weights((ow_in, on_in), (256, 128), weights_s, copies)
    lam_w, lam_n = lam_ref[0], lam_ref[1]

    barrier = pltpu.get_barrier_semaphore()
    for t in (1, 2, 3):
        pl.semaphore_signal(barrier, inc=1, device_id={"z": (z + t) % 4}, device_id_type=pl.DeviceIdType.MESH)
        pl.semaphore_signal(barrier, inc=1, device_id={"x": (x + t) % 4}, device_id_type=pl.DeviceIdType.MESH)
    rank = narrow.rank
    for k in range(1, 8):
        r = (rank + k) % 8
        pl.semaphore_signal(barrier, inc=1, device_id={"y": r // 2, "c": r % 2}, device_id_type=pl.DeviceIdType.MESH)
    local = []
    for h in (narrow, wide):
        for src, dst in h.own:
            local.append(pltpu.make_async_copy(src, dst, local_sems.at[len(local)]))
    for src, dst in weights.own:
        local.append(pltpu.make_async_copy(src, dst, local_sems.at[len(local)]))
    for c in local:
        c.start()
    pl.semaphore_wait(barrier, 13)

    wide.send_swap()
    wide.send_near()
    narrow.send_swap()
    weights.send()
    wide.clear()

    pos, tab = narrow.pos, narrow.tab
    for i, t in enumerate(SHIFTS):
        pos[i] = (4 * ((z + 4 - t) % 4) + x) * rows
        n = (x + 4 - t) % 4
        pos[4 + i] = (4 * z + n) * rows
        pos[8 + i] = (4 * (3 - z) + n) * rows + half

    def list_steps(p0, p1, k0, k1, n):
        def list_q(j, n):
            qi = 4 * p0 + j
            qp = pos[qi % 4] + (qi // 4) * TQ

            def list_k(kj, n):
                first, second = pos[4 + 2 * kj], pos[5 + 2 * kj]
                hi, lo = jnp.maximum(first, second), jnp.minimum(first, second)
                tab[0, n] = qi
                tab[1, n] = kj
                tab[2, n] = jnp.where(hi + half - 1 <= qp, 0, 1)
                return n + jnp.where(lo <= qp + TQ - 1, 1, 0)
            return lax.fori_loop(k0, k1, list_k, n)
        return lax.fori_loop(0, 4 * (p1 - p0), list_q, n)
    wide_a = list_steps(0, per, 0, 2, 0)
    wide_b = list_steps(0, per, 2, 4, wide_a)
    narrow_a = list_steps(0, per - 1, 0, 4, wide_b)
    narrow_b = list_steps(per - 1, per, 0, 4, narrow_a)
    for n in range(3):
        tab[n, narrow_b] = 0

    for c in local:
        c.wait()
    wide.relay_keys(0)
    wide.relay_queries()
    wide.pass_swap()
    narrow.send_near()
    narrow.clear()
    wide.turn_queries()
    wide.wait_values(0)
    wide.turn_values(0)

    def narrow_relays():
        narrow.relay_queries()
        narrow.relay_keys(0)
    wide.run(0, wide_a, [narrow.pass_swap, lambda: wide.relay_keys(1)], 0)
    wide.wait_values(1)
    wide.turn_values(1)
    wide.run(wide_a, wide_b, [narrow_relays, lambda: narrow.relay_keys(1)], 1)
    wide.send_stats(0)
    for b in range(2):
        narrow.wait_values(b)
    narrow.turn_queries()
    narrow.turn_values(0)
    narrow.turn_values(1)
    narrow.run(wide_b, narrow_a, [lambda: wide.mix_and_send(0, lam_w), weights.relay, lambda: wide.pass_parts(0)])
    narrow.send_stats(0)
    narrow.run(narrow_a, narrow_b, [lambda: narrow.mix_and_send(0, lam_n)])
    narrow.send_stats(1)
    wide.finish(0, lam_w)
    narrow.pass_parts(0)
    narrow.mix_and_send(1, lam_n)
    weights.last()
    narrow.finish(0, lam_n)
    narrow.pass_parts(1)
    mine = rows // 8
    width = weights_s.shape[1]

    def collect(h):
        for r in range(8):
            pl.when(r != rank)(h.from_rank(r).wait_recv)
        at = pl.multiple_of(rank * mine, mine)
        h.out[:, pl.ds(pl.multiple_of(rank * h.dv, h.dv), h.dv)] = h.heads[pl.ds(at, mine)]
    narrow.finish(1, lam_n)
    weights.wait()
    collect(wide)
    edge = 8 * wide.dv

    def project_wide(n, _):
        at = pl.ds(pl.multiple_of(n * 512, 512), 512)
        sum_s[:, at] = jnp.dot(wide.out[...], weights_s[0:edge, at], preferred_element_type=jnp.float32)
        return 0
    lax.fori_loop(0, width // 512, project_wide, 0)
    collect(narrow)

    def project(n, square):
        at = pl.ds(pl.multiple_of(n * 512, 512), 512)
        total = sum_s[:, at] + jnp.dot(narrow.out[...], weights_s[edge:, at], preferred_element_type=jnp.float32)
        stream = (total + residual_ref[:, at].astype(jnp.float32)).astype(jnp.bfloat16)
        stream_ref[:, at] = stream
        stream = stream.astype(jnp.float32)
        return square + jnp.sum(stream * stream, axis=-1, keepdims=True)
    square = lax.fori_loop(0, width // 512, project, jnp.zeros((mine, 1), jnp.float32))
    factor = lax.rsqrt(square / width + 1e-06)

    def norm(n, _):
        at = pl.ds(pl.multiple_of(n * 512, 512), 512)
        normed_ref[:, at] = (stream_ref[:, at].astype(jnp.float32) * factor * gain_ref[:, at]).astype(jnp.bfloat16)
        return 0
    lax.fori_loop(0, width // 512, norm, 0)
    for h in (narrow, wide):
        for r in range(8):
            pl.when(r != rank)(h.to_token(r).wait_send)
    for c in copies.all:
        c.wait_send()


def attention(qw, kw, vw, qn, kn, vn, lam, residual, out_w, out_n, gain):
    qw, kw, vw, qn, kn, vn = (a[:, 0] for a in (qw, kw, vw, qn, kn, vn))
    rows = qw.shape[0]
    half, mine = rows // 2, rows // 8
    total = 4 * rows
    bf16, f32 = jnp.bfloat16, jnp.float32

    def scratch(d, dv, both):
        return [
            pltpu.VMEM((4, rows, 2 * d), bf16),
            pltpu.VMEM((2, 4, half, 2 * d + dv) if both else (16, 128), bf16),
            pltpu.VMEM((2 * d, total), bf16),
            pltpu.VMEM((dv, total), bf16),
            pltpu.VMEM((2, dv, total), f32),
            pltpu.VMEM((2, total), f32),
            pltpu.VMEM((2, 8, total), f32),
            pltpu.VMEM((4, total), f32),
            pltpu.VMEM((3, 4, total), f32),
            pltpu.VMEM((4, rows, dv), bf16),
            pltpu.VMEM((3, rows, dv), bf16),
            pltpu.VMEM((2, half, dv), bf16),
            pltpu.VMEM((rows, dv), bf16),
            pltpu.VMEM((mine, 8 * dv), bf16),
        ]
    any_ = pl.BlockSpec(memory_space=pl.ANY)
    vmem = pl.BlockSpec(memory_space=pltpu.VMEM)
    count = 2 * (4 + 2 + 4 + 2 + 4 + 8) + 3 * 9 + 2 * 9
    width = residual.shape[1]
    return pl.pallas_call(
        functools.partial(attention_kernel, rows=rows),
        out_shape=(jax.ShapeDtypeStruct((mine, width), bf16),) * 2,
        in_specs=[pl.BlockSpec(memory_space=pltpu.SMEM), vmem, vmem] + [any_] * 8,
        out_specs=(vmem, vmem),
        scratch_shapes=scratch(64, 128, True) + scratch(128, 256, False) + [
            pltpu.SMEM((3, 2 * 4 * (rows // TQ) * 4 + 1), jnp.int32),
            pltpu.SMEM((12,), jnp.int32),
            pltpu.VMEM((2, rows, TQ), f32),
            pltpu.VMEM((2, rows, TQ), f32),
            pltpu.VMEM((2, 8, TQ), f32),
            pltpu.VMEM((2, 8, TQ), f32),
            pltpu.VMEM((2, rows, TQ), bf16),
            pltpu.SemaphoreType.DMA((count,)),
            pltpu.SemaphoreType.DMA((count,)),
            pltpu.SemaphoreType.DMA((8,)),
            pltpu.VMEM((8 * 384, width), bf16),
            pltpu.VMEM((mine, width), f32),
            pltpu.VMEM((4, half, 512), bf16),
            pltpu.VMEM((4, half, 512), bf16),
        ],
        name="attention",
        cost_estimate=pl.CostEstimate(flops=100 * 10**9, bytes_accessed=10**7, transcendentals=0),
        compiler_params=pltpu.CompilerParams(collective_id=0, has_side_effects=True, vmem_limit_bytes=60 * 2**20),
    )(lam.reshape(-1), residual, gain.reshape(1, -1), out_w, out_n, qn, kn, vn, qw, kw, vw)


def device_of(e):
    return {"z": e // 32, "x": (e // 8) % 4, "y": (e // 2) % 4, "c": e % 2}


def swapped(perm, rows):
    return jnp.dot(perm, rows, preferred_element_type=jnp.float32).astype(jnp.bfloat16)


def to_tiles(perm, block):
    width = block.shape[1] // 16
    stacked = jnp.concatenate([block[:, g * width:(g + 1) * width] for g in range(16)], axis=0)
    return swapped(perm, stacked).reshape(16, 16, width)


def experts_kernel(token_ref, slot_ref, weight_ref, normed_ref, stream_ref, gate_in, up_in, down_in, out_ref,
                   gate_s, up_s, down_s, perm_s, rows_s, stream_s, send_s, got_s, flat_s, hidden_s, back_s,
                   weight_sems, send_sems, recv_sems, send2_sems, recv2_sems):
    count = 128
    cap = send_s.shape[0] // count
    total = send_s.shape[0]
    tokens = normed_ref.shape[0]
    me = ((lax.axis_index("z") * 4 + lax.axis_index("x")) * 4 + lax.axis_index("y")) * 2 + lax.axis_index("c")
    loads = [
        pltpu.make_async_copy(src.at[0], dst, weight_sems.at[n])
        for n, (src, dst) in enumerate(((gate_in, gate_s), (up_in, up_s), (down_in, down_s)))
    ]
    for c in loads:
        c.start()
    barrier = pltpu.get_barrier_semaphore()

    def greet(k, _):
        pl.semaphore_signal(barrier, inc=1, device_id=device_of((me + k) % count), device_id_type=pl.DeviceIdType.MESH)
        return 0
    lax.fori_loop(1, count, greet, 0)

    r = lax.broadcasted_iota(jnp.int32, (256, 256), 0)
    c = lax.broadcasted_iota(jnp.int32, (256, 256), 1)
    perm_s[...] = jnp.where((r % 16) * 16 + r // 16 == c, 1.0, 0.0).astype(jnp.bfloat16)
    perm = perm_s[...]
    for b in range(tokens // 16):
        s = slice(b * 16, (b + 1) * 16)
        rows_s[s] = to_tiles(perm, normed_ref[s])

    def fill(n, _):
        for u in range(8):
            send_s[n * 8 + u] = rows_s[token_ref[n * 8 + u]]
        return 0
    lax.fori_loop(0, total // 8, fill, 0)
    pl.semaphore_wait(barrier, count - 1)

    def copy(src, dst, sends, recvs, k):
        e = (me + k) % count
        return pltpu.make_async_remote_copy(
            src_ref=src.at[pl.ds(e * cap, cap)],
            dst_ref=dst.at[pl.ds(me * cap, cap)],
            send_sem=sends.at[k],
            recv_sem=recvs.at[k],
            device_id=device_of(e),
            device_id_type=pl.DeviceIdType.MESH,
        )

    def exchange(src, dst, sends, recvs):
        def go(k, _):
            copy(src, dst, sends, recvs, (k * 53) % 128).start()
            return 0
        lax.fori_loop(1, count, go, 0)
        dst[pl.ds(me * cap, cap)] = src[pl.ds(me * cap, cap)]

    def arrive(src, dst, sends, recvs):
        def done(k, _):
            copy(src, dst, sends, recvs, k).wait_recv()
            return 0
        lax.fori_loop(1, count, done, 0)

    def leave(src, dst, sends, recvs):
        def done(k, _):
            copy(src, dst, sends, recvs, k).wait_send()
            return 0
        lax.fori_loop(1, count, done, 0)

    there = (send_s, got_s, send_sems, recv_sems)
    exchange(*there)
    for b in range(tokens // 16):
        s = slice(b * 16, (b + 1) * 16)
        stream_s[s] = to_tiles(perm, stream_ref[s])
    for c in loads:
        c.wait()
    arrive(*there)

    def flatten(n, _):
        for u in range(4):
            at = pl.multiple_of((n * 4 + u) * 16, 16)
            turned = swapped(perm, got_s[pl.ds(at, 16)].reshape(256, 128))
            for g in range(16):
                flat_s[pl.ds(at, 16), g * 128:(g + 1) * 128] = turned[g * 16:(g + 1) * 16]
        return 0
    lax.fori_loop(0, total // 64, flatten, 0)

    def first(n, _):
        at = pl.ds(pl.multiple_of(n * 256, 256), 256)
        gate = jnp.dot(flat_s[...], gate_s[:, at], preferred_element_type=jnp.float32)
        up = jnp.dot(flat_s[...], up_s[:, at], preferred_element_type=jnp.float32)
        hidden_s[:, at] = (gate * jax.nn.sigmoid(gate) * up).astype(jnp.bfloat16)
        return 0
    lax.fori_loop(0, hidden_s.shape[1] // 256, first, 0)

    def second(n, _):
        at = pl.ds(pl.multiple_of(n * 256, 256), 256)
        flat_s[:, at] = jnp.dot(hidden_s[...], down_s[:, at], preferred_element_type=jnp.float32).astype(jnp.bfloat16)
        return 0
    lax.fori_loop(0, flat_s.shape[1] // 256, second, 0)
    leave(*there)

    def unflatten(n, _):
        for u in range(4):
            at = pl.ds(pl.multiple_of((n * 4 + u) * 16, 16), 16)
            send_s[at] = to_tiles(perm, flat_s[at, :])
        return 0
    lax.fori_loop(0, total // 64, unflatten, 0)

    back = (send_s, back_s, send2_sems, recv2_sems)
    exchange(*back)
    arrive(*back)

    def combine(n, _):
        for u in range(4):
            t = n * 4 + u
            summed = weight_ref[2 * t] * back_s[slot_ref[2 * t]].astype(jnp.float32)
            summed = summed + weight_ref[2 * t + 1] * back_s[slot_ref[2 * t + 1]].astype(jnp.float32)
            rows_s[t] = (stream_s[t].astype(jnp.float32) + summed).astype(jnp.bfloat16)
        return 0
    lax.fori_loop(0, tokens // 4, combine, 0)
    for b in range(tokens // 16):
        s = slice(b * 16, (b + 1) * 16)
        turned = swapped(perm, rows_s[s].reshape(256, 128))
        for g in range(16):
            out_ref[s, g * 128:(g + 1) * 128] = turned[g * 16:(g + 1) * 16]
    leave(*back)


def experts(token_of_slot, slot_of_token, weight, normed, stream, gate, up, down):
    tokens, width = normed.shape
    slots = token_of_slot.shape[0]
    inner = gate.shape[2]
    smem = pl.BlockSpec(memory_space=pltpu.SMEM)
    vmem = pl.BlockSpec(memory_space=pltpu.VMEM)
    any_ = pl.BlockSpec(memory_space=pl.ANY)
    bf16 = jnp.bfloat16
    return pl.pallas_call(
        experts_kernel,
        out_shape=jax.ShapeDtypeStruct((tokens, width), bf16),
        in_specs=[smem] * 3 + [vmem] * 2 + [any_] * 3,
        out_specs=vmem,
        scratch_shapes=[
            pltpu.VMEM((width, inner), bf16),
            pltpu.VMEM((width, inner), bf16),
            pltpu.VMEM((inner, width), bf16),
            pltpu.VMEM((256, 256), bf16),
            pltpu.VMEM((tokens, 16, width // 16), bf16),
            pltpu.VMEM((tokens, 16, width // 16), bf16),
            pltpu.VMEM((slots, 16, width // 16), bf16),
            pltpu.VMEM((slots, 16, width // 16), bf16),
            pltpu.VMEM((slots, width), bf16),
            pltpu.VMEM((slots, inner), bf16),
            pltpu.VMEM((slots, 16, width // 16), bf16),
            pltpu.SemaphoreType.DMA((3,)),
            pltpu.SemaphoreType.DMA((128,)),
            pltpu.SemaphoreType.DMA((128,)),
            pltpu.SemaphoreType.DMA((128,)),
            pltpu.SemaphoreType.DMA((128,)),
        ],
        name="experts",
        cost_estimate=pl.CostEstimate(flops=50 * 10**9, bytes_accessed=2 * 10**7, transcendentals=0),
        compiler_params=pltpu.CompilerParams(collective_id=1, has_side_effects=True, vmem_limit_bytes=60 * 2**20),
    )(token_of_slot, slot_of_token, weight, normed, stream, gate, up, down)


def shards(
    query_wide,
    key_wide,
    value_wide,
    query_narrow,
    key_narrow,
    value_narrow,
    mix_lambda,
    residual_in,
    out_wide,
    out_narrow,
    ffn_gain,
    expert_ids,
    expert_weights,
    gate_weight,
    up_weight,
    down_weight,
):
    tok_count, local_heads, _ = query_wide.shape
    stream, normed = attention(
        query_wide, key_wide, value_wide, query_narrow, key_narrow, value_narrow, mix_lambda,
        residual_in, out_wide, out_narrow, ffn_gain,
    )
    tp_size = lax.axis_size(TP)
    local_rows = tok_count // tp_size
    experts_all = lax.axis_size(SP) * tp_size
    capacity = max(2, 4 * local_rows // experts_all)
    flat_expert = expert_ids.reshape(-1)
    expert_hot = (flat_expert[:, None] == jnp.arange(experts_all, dtype=jnp.int32)[None, :]).astype(
        jnp.int32
    )
    slot_rank = jnp.sum((jnp.cumsum(expert_hot, axis=0) - 1) * expert_hot, axis=1)
    flat_slot = flat_expert * capacity + slot_rank
    slot_ids = jnp.arange(experts_all * capacity, dtype=jnp.int32)
    placed = slot_ids[:, None] == flat_slot[None, :]
    token = jnp.arange(2 * local_rows, dtype=jnp.int32) // 2
    token_of_slot = jnp.max(jnp.where(placed, token[None, :], 0), axis=1)
    return experts(
        token_of_slot, flat_slot, expert_weights.reshape(-1), normed, stream, gate_weight, up_weight, down_weight
    )


def solution(mesh):
    finer = Mesh(mesh.devices.reshape(4, 4, 4, 2), ("z", "x", "y", "c"))
    placed = (
        P(SP, TP, None),
        P(SP, TP, None),
        P(SP, TP, None),
        P(SP, TP, None),
        P(SP, TP, None),
        P(SP, TP, None),
        P(None, TP),
        P(SP_TP, None),
        P(TP, None),
        P(TP, None),
        P(),
        P(SP_TP, None),
        P(SP_TP, None),
        P(SP_TP, None, None),
        P(SP_TP, None, None),
        P(SP_TP, None, None),
    )
    return jax.shard_map(
        shards, mesh=finer, in_specs=placed, out_specs=P(SP_TP, None), check_vma=False
    )
```

time: 234 us -> 191 us (0.82)
  Pallas kernels: 200 us -> 185 us
  between operations: 13.6 us -> 0.07 us
  matrix products: 8.17 us -> 0 us
  other arithmetic: 5 us -> 1.2 us
    pallas_call x1, Pallas kernels: 87.5 us -> 78.2 us  [experts(): pl.pallas_call(experts_kernel, out_shape=jax.ShapeDtypeStruct((tokens, wi...]
    dot_general x2 -> x0, matrix products: 8.17 us -> none  [the longest x1 5.02 us: shards(): jnp.dot(mine_wide, whole_wide, preferred_element_type=jnp.float32)]
    pallas_call x1, Pallas kernels: 112 us -> 107 us  [attention(): pl.pallas_call(functools.partial(attention_kernel, rows=rows), out_shape=...]
    concatenate x2 -> x0, other arithmetic: 2.88 us -> none  [the longest x1 2.09 us: attention(): jnp.concatenate([kw, vw], axis=1)]
    unnamed x19 -> x6, local copies, waits for them, and re-layouts: 4.68 us -> 3.33 us
  transfers between devices with their start and end apart: 2 -> 0, of which waited for: 0 -> 0; matrix products, arithmetic and copies ran while one was open for 6% -> 0% of each run, Pallas kernels for 48% -> 0%
where the time goes in v4:
time: 191 us
  Pallas kernels  185 us (97%)
  local copies, waits for them, and re-layouts  4.19 us (2%)
    pallas_call x1, Pallas kernels, attention(): pl.pallas_call(functools.partial(attention_kernel, rows=rows), out_shape=...  107 us
    pallas_call x1, Pallas kernels, experts(): pl.pallas_call(experts_kernel, out_shape=jax.ShapeDtypeStruct((tokens, wi...  78.2 us

profile of v4, /device:TPU:1, one launch (start us, length us, event | category | flops | bytes accessed | tf_op | source)
XLA Modules:
  0.0 190.7 jit_solution(142968752312735662)
XLA Ops:
  0.0 0.8 copy.21
  0.8 0.1 reshape.45
  0.9 0.1 iota_compare_fusion.1
  1.0 0.8 copy.24
  1.8 0.7 reshape.48.weight_ref
  2.5 0.1 fusion
  2.7 0.2 fusion.3
  2.9 0.0 copy-start
  3.0 0.7 select_reduce_fusion.token_ref
  3.7 107.0 %attention.1 = (bf16[96,2048]{1,0:T(8,128)(2,1)}, bf16[96,2048]{1,0:T(8,128)(2,1)}) custom-call(f32[2]{0:T(128)} %bitcast.29, bf16[96,2048]{1,0:T(8,128)(2,1)} %residual_ref.1, f32[1,2048]{1,0:T(1,128)} %bitcast.28, bf16[256,2048]{1,0:T(8,128)(2,1)} %ow_in.1, bf16[128,2048]{1,0:T(8,128)(2,1)} %on_in.1, bf16[768,128]{1,0:T(8,128)(2,1)} %bitcast.25, ...), custom_call_target="tpu_custom_call" | custom-call | flops 99999997952 | bytes 10000000 | tf_op jit(solution)/shard_map/attention/pallas_call | solution.py:538
  110.7 0.0 copy-done
  110.7 78.2 %experts.1 = bf16[96,2048]{1,0:T(8,128)(2,1)} custom-call(s32[384]{0:T(512)} %select_reduce_fusion.token_ref, s32[192]{0:T(256)} %copy-done, f32[192]{0:T(256)} %reshape.48.weight_ref, bf16[96,2048]{1,0:T(8,128)(2,1)} %get-tuple-element.7.normed_ref, bf16[96,2048]{1,0:T(8,128)(2,1)} %get-tuple-element.8.stream_ref, bf16[1,2048,1024]{2,1,0:T(8,128)(2,1)} %gate_in.1, ...), custom_call_target="tpu_custom_call" | custom-call | flops 49999998976 | bytes 20000000 | tf_op jit(solution)/shard_map/experts/pallas_call | solution.py:713
  188.9 1.8 copy.28
  (8 shorter events, 0.1 us)
Async XLA Ops:
  2.9 107.7 %copy-start = (s32[192]{0:T(256)}, s32[192]{0:T(256)S(1)}, u32[]{:S(2)}) copy-start(s32[192]{0:T(256)S(1)} %get-tuple-element.10.slot_ref) | copy-start | bytes 2308

commit v5 on v4

--- a/solution.py
+++ b/solution.py
@@ -473,7 +473,6 @@
             pl.when(r != rank)(h.from_rank(r).wait_recv)
         at = pl.multiple_of(rank * mine, mine)
         h.out[:, pl.ds(pl.multiple_of(rank * h.dv, h.dv), h.dv)] = h.heads[pl.ds(at, mine)]
-    narrow.finish(1, lam_n)
     weights.wait()
     collect(wide)
     edge = 8 * wide.dv
@@ -483,6 +482,7 @@
         sum_s[:, at] = jnp.dot(wide.out[...], weights_s[0:edge, at], preferred_element_type=jnp.float32)
         return 0
     lax.fori_loop(0, width // 512, project_wide, 0)
+    narrow.finish(1, lam_n)
     collect(narrow)
 
     def project(n, square):
@@ -577,13 +577,16 @@
 
 
 def experts_kernel(token_ref, slot_ref, weight_ref, normed_ref, stream_ref, gate_in, up_in, down_in, out_ref,
-                   gate_s, up_s, down_s, perm_s, rows_s, stream_s, send_s, got_s, flat_s, hidden_s, back_s,
-                   weight_sems, send_sems, recv_sems, send2_sems, recv2_sems):
+                   gate_s, up_s, down_s, perm_s, rows_s, stream_s, send_s, got_a, got_b, flat_s, hidden_s, ret_a, ret_b, back_s,
+                   weight_sems, send_sems, recv_sems):
     count = 128
     cap = send_s.shape[0] // count
     total = send_s.shape[0]
+    part = total // 2
     tokens = normed_ref.shape[0]
     me = ((lax.axis_index("z") * 4 + lax.axis_index("x")) * 4 + lax.axis_index("y")) * 2 + lax.axis_index("c")
+    chip, core = me // 2, me % 2
+    got, ret = (got_a, got_b), (ret_a, ret_b)
     loads = [
         pltpu.make_async_copy(src.at[0], dst, weight_sems.at[n])
         for n, (src, dst) in enumerate(((gate_in, gate_s), (up_in, up_s), (down_in, down_s)))
@@ -612,79 +615,75 @@
     lax.fori_loop(0, total // 8, fill, 0)
     pl.semaphore_wait(barrier, count - 1)
 
-    def copy(src, dst, sends, recvs, k):
-        e = (me + k) % count
+    def peer(h, j):
+        other = (chip + j) % 64
+        return other, other * 2 + (core if h == 0 else 1 - core)
+
+    def remote(src, dst, way, n, e):
         return pltpu.make_async_remote_copy(
-            src_ref=src.at[pl.ds(e * cap, cap)],
-            dst_ref=dst.at[pl.ds(me * cap, cap)],
-            send_sem=sends.at[k],
-            recv_sem=recvs.at[k],
-            device_id=device_of(e),
-            device_id_type=pl.DeviceIdType.MESH,
+            src_ref=src, dst_ref=dst, send_sem=send_sems.at[way, n], recv_sem=recv_sems.at[way, n],
+            device_id=device_of(e), device_id_type=pl.DeviceIdType.MESH,
         )
 
-    def exchange(src, dst, sends, recvs):
-        def go(k, _):
-            copy(src, dst, sends, recvs, (k * 53) % 128).start()
-            return 0
-        lax.fori_loop(1, count, go, 0)
-        dst[pl.ds(me * cap, cap)] = src[pl.ds(me * cap, cap)]
-
-    def arrive(src, dst, sends, recvs):
-        def done(k, _):
-            copy(src, dst, sends, recvs, k).wait_recv()
-            return 0
-        lax.fori_loop(1, count, done, 0)
-
-    def leave(src, dst, sends, recvs):
-        def done(k, _):
-            copy(src, dst, sends, recvs, k).wait_send()
-            return 0
-        lax.fori_loop(1, count, done, 0)
-
-    there = (send_s, got_s, send_sems, recv_sems)
-    exchange(*there)
+    def there(h, j):
+        _, e = peer(h, j)
+        return remote(send_s.at[pl.ds(e * cap, cap)], got[h].at[pl.ds(chip * cap, cap)], 0, h * 64 + j, e)
+
+    def back(h, j):
+        other, e = peer(h, j)
+        return remote(ret[h].at[pl.ds(other * cap, cap)], back_s.at[pl.ds(me * cap, cap)], 1, h * 64 + j, e)
+
+    def each(h, act):
+        def go(n, _):
+            act(h, (n * 27) % 64)
+            return 0
+        lax.fori_loop(1 - h, 64, go, 0)
+
+    each(0, lambda h, j: there(h, j).start())
+    got_a[pl.ds(chip * cap, cap)] = send_s[pl.ds(me * cap, cap)]
+    each(1, lambda h, j: there(h, j).start())
     for b in range(tokens // 16):
         s = slice(b * 16, (b + 1) * 16)
         stream_s[s] = to_tiles(perm, stream_ref[s])
     for c in loads:
         c.wait()
-    arrive(*there)
-
-    def flatten(n, _):
-        for u in range(4):
-            at = pl.multiple_of((n * 4 + u) * 16, 16)
-            turned = swapped(perm, got_s[pl.ds(at, 16)].reshape(256, 128))
-            for g in range(16):
-                flat_s[pl.ds(at, 16), g * 128:(g + 1) * 128] = turned[g * 16:(g + 1) * 16]
-        return 0
-    lax.fori_loop(0, total // 64, flatten, 0)
-
-    def first(n, _):
-        at = pl.ds(pl.multiple_of(n * 256, 256), 256)
-        gate = jnp.dot(flat_s[...], gate_s[:, at], preferred_element_type=jnp.float32)
-        up = jnp.dot(flat_s[...], up_s[:, at], preferred_element_type=jnp.float32)
-        hidden_s[:, at] = (gate * jax.nn.sigmoid(gate) * up).astype(jnp.bfloat16)
-        return 0
-    lax.fori_loop(0, hidden_s.shape[1] // 256, first, 0)
-
-    def second(n, _):
-        at = pl.ds(pl.multiple_of(n * 256, 256), 256)
-        flat_s[:, at] = jnp.dot(hidden_s[...], down_s[:, at], preferred_element_type=jnp.float32).astype(jnp.bfloat16)
-        return 0
-    lax.fori_loop(0, flat_s.shape[1] // 256, second, 0)
-    leave(*there)
-
-    def unflatten(n, _):
-        for u in range(4):
-            at = pl.ds(pl.multiple_of((n * 4 + u) * 16, 16), 16)
-            send_s[at] = to_tiles(perm, flat_s[at, :])
-        return 0
-    lax.fori_loop(0, total // 64, unflatten, 0)
-
-    back = (send_s, back_s, send2_sems, recv2_sems)
-    exchange(*back)
-    arrive(*back)
+
+    for h in range(2):
+        each(h, lambda h, j: there(h, j).wait_recv())
+
+        def flatten(n, _):
+            for u in range(4):
+                at = pl.multiple_of((n * 4 + u) * 16, 16)
+                turned = swapped(perm, got[h][pl.ds(at, 16)].reshape(256, 128))
+                for g in range(16):
+                    flat_s[pl.ds(at, 16), g * 128:(g + 1) * 128] = turned[g * 16:(g + 1) * 16]
+            return 0
+        lax.fori_loop(0, part // 64, flatten, 0)
+
+        def first(n, _):
+            at = pl.ds(pl.multiple_of(n * 256, 256), 256)
+            gate = jnp.dot(flat_s[...], gate_s[:, at], preferred_element_type=jnp.float32)
+            up = jnp.dot(flat_s[...], up_s[:, at], preferred_element_type=jnp.float32)
+            hidden_s[:, at] = (gate * jax.nn.sigmoid(gate) * up).astype(jnp.bfloat16)
+            return 0
+        lax.fori_loop(0, hidden_s.shape[1] // 256, first, 0)
+
+        def second(n, _):
+            at = pl.ds(pl.multiple_of(n * 256, 256), 256)
+            flat_s[:, at] = jnp.dot(hidden_s[...], down_s[:, at], preferred_element_type=jnp.float32).astype(jnp.bfloat16)
+            return 0
+        lax.fori_loop(0, flat_s.shape[1] // 256, second, 0)
+
+        def unflatten(n, _):
+            for u in range(4):
+                at = pl.ds(pl.multiple_of((n * 4 + u) * 16, 16), 16)
+                ret[h][at] = to_tiles(perm, flat_s[at, :])
+            return 0
+        lax.fori_loop(0, part // 64, unflatten, 0)
+        each(h, lambda h, j: back(h, j).start())
+    back_s[pl.ds(me * cap, cap)] = ret_a[pl.ds(chip * cap, cap)]
+    for h in range(2):
+        each(h, lambda h, j: back(h, j).wait_recv())
 
     def combine(n, _):
         for u in range(4):
@@ -699,7 +698,9 @@
         turned = swapped(perm, rows_s[s].reshape(256, 128))
         for g in range(16):
             out_ref[s, g * 128:(g + 1) * 128] = turned[g * 16:(g + 1) * 16]
-    leave(*back)
+    for h in range(2):
+        each(h, lambda h, j: there(h, j).wait_send())
+        each(h, lambda h, j: back(h, j).wait_send())
 
 
 def experts(token_of_slot, slot_of_token, weight, normed, stream, gate, up, down):
@@ -723,15 +724,16 @@
             pltpu.VMEM((tokens, 16, width // 16), bf16),
             pltpu.VMEM((tokens, 16, width // 16), bf16),
             pltpu.VMEM((slots, 16, width // 16), bf16),
-            pltpu.VMEM((slots, 16, width // 16), bf16),
-            pltpu.VMEM((slots, width), bf16),
-            pltpu.VMEM((slots, inner), bf16),
+            pltpu.VMEM((slots // 2, 16, width // 16), bf16),
+            pltpu.VMEM((slots // 2, 16, width // 16), bf16),
+            pltpu.VMEM((slots // 2, width), bf16),
+            pltpu.VMEM((slots // 2, inner), bf16),
+            pltpu.VMEM((slots // 2, 16, width // 16), bf16),
+            pltpu.VMEM((slots // 2, 16, width // 16), bf16),
             pltpu.VMEM((slots, 16, width // 16), bf16),
             pltpu.SemaphoreType.DMA((3,)),
-            pltpu.SemaphoreType.DMA((128,)),
-            pltpu.SemaphoreType.DMA((128,)),
-            pltpu.SemaphoreType.DMA((128,)),
-            pltpu.SemaphoreType.DMA((128,)),
+            pltpu.SemaphoreType.DMA((2, 128)),
+            pltpu.SemaphoreType.DMA((2, 128)),
         ],
         name="experts",
         cost_estimate=pl.CostEstimate(flops=50 * 10**9, bytes_accessed=2 * 10**7, transcendentals=0),

time: 191 us -> 182 us (0.953)
  Pallas kernels: 185 us -> 174 us
    pallas_call x1, Pallas kernels: 78.2 us -> 67.2 us  [experts(): pl.pallas_call(experts_kernel, out_shape=jax.ShapeDtypeStruct((tokens, wi...]
where the time goes in v5:
time: 182 us; the launch traced here: 180 us
  Pallas kernels  174 us (96%)
  local copies, waits for them, and re-layouts  4.19 us (2%)
    pallas_call x1, Pallas kernels, attention(): pl.pallas_call(functools.partial(attention_kernel, rows=rows), out_shape=...  107 us
    pallas_call x1, Pallas kernels, experts(): pl.pallas_call(experts_kernel, out_shape=jax.ShapeDtypeStruct((tokens, wi...  67.2 us

profile of v5, /device:TPU:1, one launch (start us, length us, event | category | flops | bytes accessed | tf_op | source)
XLA Modules:
  0.0 179.9 jit_solution(17256592247270485385)
XLA Ops:
  0.0 0.8 copy.21
  0.8 0.1 reshape.45
  0.9 0.1 iota_compare_fusion.1
  1.0 0.8 copy.24
  1.8 0.7 reshape.48.weight_ref
  2.5 0.1 fusion
  2.7 0.2 fusion.3
  2.9 0.0 copy-start
  3.0 0.7 select_reduce_fusion.token_ref
  3.7 107.2 %attention.1 = (bf16[96,2048]{1,0:T(8,128)(2,1)}, bf16[96,2048]{1,0:T(8,128)(2,1)}) custom-call(f32[2]{0:T(128)} %bitcast.29, bf16[96,2048]{1,0:T(8,128)(2,1)} %residual_ref.1, f32[1,2048]{1,0:T(1,128)} %bitcast.28, bf16[256,2048]{1,0:T(8,128)(2,1)} %ow_in.1, bf16[128,2048]{1,0:T(8,128)(2,1)} %on_in.1, bf16[768,128]{1,0:T(8,128)(2,1)} %bitcast.25, ...), custom_call_target="tpu_custom_call" | custom-call | flops 99999997952 | bytes 10000000 | tf_op jit(solution)/shard_map/attention/pallas_call | solution.py:538
  110.9 0.0 copy-done
  110.9 67.2 %experts.1 = bf16[96,2048]{1,0:T(8,128)(2,1)} custom-call(s32[384]{0:T(512)} %select_reduce_fusion.token_ref, s32[192]{0:T(256)} %copy-done, f32[192]{0:T(256)} %reshape.48.weight_ref, bf16[96,2048]{1,0:T(8,128)(2,1)} %get-tuple-element.7.normed_ref, bf16[96,2048]{1,0:T(8,128)(2,1)} %get-tuple-element.8.stream_ref, bf16[1,2048,1024]{2,1,0:T(8,128)(2,1)} %gate_in.1, ...), custom_call_target="tpu_custom_call" | custom-call | flops 49999998976 | bytes 20000000 | tf_op jit(solution)/shard_map/experts/pallas_call | solution.py:714
  178.1 1.8 copy.28
  (8 shorter events, 0.1 us)
Async XLA Ops:
  2.9 107.9 %copy-start = (s32[192]{0:T(256)}, s32[192]{0:T(256)S(1)}, u32[]{:S(2)}) copy-start(s32[192]{0:T(256)S(1)} %get-tuple-element.10.slot_ref) | copy-start | bytes 2308

commit v6 on v5

--- a/solution.py
+++ b/solution.py
@@ -635,7 +635,7 @@
 
     def each(h, act):
         def go(n, _):
-            act(h, (n * 27) % 64)
+            act(h, (n * 37) % 64)
             return 0
         lax.fori_loop(1 - h, 64, go, 0)
 

time: 182 us -> 181 us (level)
  no operation moved by 1% of the time
where the time goes in v6:
time: 181 us
  Pallas kernels  175 us (97%)
  local copies, waits for them, and re-layouts  4.19 us (2%)
    pallas_call x1, Pallas kernels, attention(): pl.pallas_call(functools.partial(attention_kernel, rows=rows), out_shape=...  107 us
    pallas_call x1, Pallas kernels, experts(): pl.pallas_call(experts_kernel, out_shape=jax.ShapeDtypeStruct((tokens, wi...  67.9 us

profile of v6, /device:TPU:1, one launch (start us, length us, event | category | flops | bytes accessed | tf_op | source)
XLA Modules:
  0.0 180.6 jit_solution(12949315575221881386)
XLA Ops:
  0.0 0.8 copy.21
  0.8 0.1 reshape.45
  0.9 0.1 iota_compare_fusion.1
  1.0 0.8 copy.24
  1.8 0.7 reshape.48.weight_ref
  2.5 0.1 fusion
  2.7 0.2 fusion.3
  2.9 0.0 copy-start
  3.0 0.7 select_reduce_fusion.token_ref
  3.7 107.2 %attention.1 = (bf16[96,2048]{1,0:T(8,128)(2,1)}, bf16[96,2048]{1,0:T(8,128)(2,1)}) custom-call(f32[2]{0:T(128)} %bitcast.29, bf16[96,2048]{1,0:T(8,128)(2,1)} %residual_ref.1, f32[1,2048]{1,0:T(1,128)} %bitcast.28, bf16[256,2048]{1,0:T(8,128)(2,1)} %ow_in.1, bf16[128,2048]{1,0:T(8,128)(2,1)} %on_in.1, bf16[768,128]{1,0:T(8,128)(2,1)} %bitcast.25, ...), custom_call_target="tpu_custom_call" | custom-call | flops 99999997952 | bytes 10000000 | tf_op jit(solution)/shard_map/attention/pallas_call | solution.py:538
  110.9 0.0 copy-done
  110.9 67.9 %experts.1 = bf16[96,2048]{1,0:T(8,128)(2,1)} custom-call(s32[384]{0:T(512)} %select_reduce_fusion.token_ref, s32[192]{0:T(256)} %copy-done, f32[192]{0:T(256)} %reshape.48.weight_ref, bf16[96,2048]{1,0:T(8,128)(2,1)} %get-tuple-element.7.normed_ref, bf16[96,2048]{1,0:T(8,128)(2,1)} %get-tuple-element.8.stream_ref, bf16[1,2048,1024]{2,1,0:T(8,128)(2,1)} %gate_in.1, ...), custom_call_target="tpu_custom_call" | custom-call | flops 49999998976 | bytes 20000000 | tf_op jit(solution)/shard_map/experts/pallas_call | solution.py:714
  178.8 1.8 copy.28
  (8 shorter events, 0.1 us)
Async XLA Ops:
  2.9 107.9 %copy-start = (s32[192]{0:T(256)}, s32[192]{0:T(256)S(1)}, u32[]{:S(2)}) copy-start(s32[192]{0:T(256)S(1)} %get-tuple-element.10.slot_ref) | copy-start | bytes 2308
